TPU v7x, 32 devices: a whole 2x2x4 slice. The times are simulated.
32 devices in a mesh: sp: 8 (over z, y), tp: 4 (over x, core).
Axes of the slice: x: 2, y: 2, z: 4, core: 2. Of those that a mesh axis runs over, the one named last changes fastest.
Arguments:
- inputs: bfloat16 [2, 1024, 2048], P(None, 'sp'), may hold values from -6 to 6
- norm_gain: float32 [2048], replicated, may hold values from 0.1 to 1.9
- query_weight: bfloat16 [2048, 1024], P('sp', 'tp'), may hold values from -0.125 to 0.125
- key_weight: bfloat16 [2048, 256], P('sp', 'tp'), may hold values from -0.125 to 0.125
- value_weight: bfloat16 [2048, 256], P('sp', 'tp'), may hold values from -0.125 to 0.125
- query_gain: float32 [64], replicated, may hold values from 0.1 to 24
- key_gain: float32 [64], replicated, may hold values from 0.1 to 1.9
- forget_cache: float32 [2, 16, 1024], P(None, 'tp'), may hold values from -104 to 0, as said below
- rec_in_weight: bfloat16 [2048, 1024], P('sp', 'tp'), may hold values from -0.125 to 0.125
- rec_gate_weight: bfloat16 [2048, 1024], P('sp', 'tp'), may hold values from -0.125 to 0.125
- conv_weight: bfloat16 [4, 1024], P(None, 'tp'), may hold values from -3 to 3
- decay_gate_weight: bfloat16 [16, 64, 64], P('tp'), may hold values from -0.75 to 0.75
- input_gate_weight: bfloat16 [16, 64, 64], P('tp'), may hold values from -0.75 to 0.75
- decay_param: float32 [1024], P('tp'), may hold values from 4 to 16
- decay_extra: float32 [2, 1024, 1024], P(None, 'sp', 'tp'), may hold values from -2 to 0
- attn_out_gain: float32 [1024], P('tp'), may hold values from 0.1 to 1.9
- rec_out_gain: float32 [1024], P('tp'), may hold values from 0.1 to 1.9
- out_att_weight: bfloat16 [1024, 2048], P('tp'), may hold values from -0.125 to 0.125
- out_rec_weight: bfloat16 [1024, 2048], P('tp'), may hold values from -0.125 to 0.125
Outputs:
- mixed: bfloat16 [2, 1024, 2048], P(None, 'sp', 'tp')
Inputs may be any that keep to these rules, and one draw needn't show every extreme that they name: `forget_cache`: Non-increasing along the positions of each sequence and head.
All inputs are finite; a program needn't handle non-finite values.
Results may differ from a plain program's by a relative error of at most 0.012.
The roundings to bfloat16 on the way count: a program that leaves them out, or rounds other values in their place, can miss the bound.
Values may be sent and summed in bfloat16 or wider, within the bound.
No kernel may reach another device: no remote copies, remote signals or barrier semaphores. Data moves between devices by JAX's collectives and lax.ppermute only.
A program may use at most 128 MiB of HBM per device.

v0:
```python
import functools

import jax
import jax.numpy as jnp
from jax import lax
from jax.experimental import pallas as pl
from jax.experimental.pallas import tpu as pltpu
from jax.sharding import PartitionSpec as P

D = 2048
LRU_BLOCK = 64
CONV_TAPS = 4


lru_const = 8.0
norm_eps = 1e-06


def from_behind(value, axis, steps):
    count = lax.axis_size(axis)
    leading, last = (max(0, -steps), min(count, count - steps))
    return lax.ppermute(value, axis, [(source, source + steps) for source in range(leading, last)])


def rms_scale(values, gain):
    multiplier = lax.rsqrt(jnp.mean(values * values, axis=-1, keepdims=True) + norm_eps)
    return values * multiplier * gain


def merge_state(earlier, later):
    return (earlier[0] * later[0], later[0] * earlier[1] + later[1])


def block_length(length, span):
    shards = max(length // span, 1)
    group_size = 1
    for trial_size in range(1, shards + 1):
        if shards % trial_size == 0 and trial_size * span <= 1024:
            group_size = trial_size
    sub_size = group_size * span
    if length % sub_size:
        sub_size = length
    return sub_size


def body(
    inputs,
    norm_gain,
    query_weight,
    key_weight,
    value_weight,
    query_gain,
    key_gain,
    forget_cache,
    rec_in_weight,
    rec_gate_weight,
    conv_weight,
    decay_gate_weight,
    input_gate_weight,
    decay_param,
    decay_extra,
    attn_out_gain,
    rec_out_gain,
    out_att_weight,
    out_rec_weight,
):
    seq_count, seq_span, model_width = inputs.shape
    row_count = seq_count * seq_span
    head_dim = query_gain.shape[0]
    att_local = query_weight.shape[1] // head_dim
    kv_local = key_weight.shape[1] // head_dim
    head_group = att_local // kv_local
    channels = rec_in_weight.shape[1]
    normed = rms_scale(
        inputs.reshape(row_count, model_width).astype(jnp.float32), norm_gain
    ).astype(jnp.bfloat16)
    normed_cols = normed.T
    row_contract = (((0,), (0,)), ((), ()))
    kv_cols = key_weight.shape[1]
    pieces = (
        lax.all_gather(query_weight, "sp", axis=0, tiled=True),
        lax.all_gather(key_weight, "sp", axis=0, tiled=True),
        lax.all_gather(value_weight, "sp", axis=0, tiled=True),
        lax.all_gather(rec_in_weight, "sp", axis=0, tiled=True),
        lax.all_gather(rec_gate_weight, "sp", axis=0, tiled=True),
    )
    query_proj, key_proj, value_sum, rec_in_sum, gate_proj = tuple(
        (
            lax.dot_general(
                normed_cols, weight_part, row_contract, preferred_element_type=jnp.float32
            )
            for weight_part in pieces
        )
    )
    queries = rms_scale(query_proj.reshape(row_count, att_local, head_dim), query_gain).astype(
        jnp.bfloat16
    )
    queries = queries.reshape(seq_count, seq_span, kv_local, head_group, head_dim).transpose(
        0, 2, 3, 1, 4
    )
    queries = queries.reshape(seq_count, kv_local, head_group * seq_span, head_dim)
    key_heads = rms_scale(key_proj.reshape(row_count, kv_local, head_dim), key_gain).astype(
        jnp.bfloat16
    )
    key_heads = key_heads.reshape(seq_count, seq_span, kv_cols)
    value_heads = value_sum.astype(jnp.bfloat16).reshape(seq_count, seq_span, kv_cols)
    key_value = jnp.concatenate([key_heads, value_heads], axis=2)
    my_first = lax.axis_index("sp") * seq_span
    own_gates = lax.dynamic_slice_in_dim(forget_cache, my_first, seq_span, 2)
    own_gates = own_gates.reshape(seq_count, kv_local, head_group, seq_span, 1)
    query_pos = my_first + jnp.tile(jnp.arange(seq_span, dtype=jnp.int32), head_group)
    scaling = head_dim ** (-0.5)
    start_state = (
        jnp.full((seq_count, kv_local, head_group * seq_span), -jnp.inf, jnp.float32),
        jnp.zeros((seq_count, kv_local, head_group * seq_span), jnp.float32),
        jnp.zeros((seq_count, kv_local, head_group * seq_span, head_dim), jnp.float32),
    )
    shard_part = lax.all_gather(key_value, "sp", axis=1, tiled=True)
    offset = jnp.int32(0)
    length = shard_part.shape[1]
    sub_size = block_length(length, seq_span)

    def one_step(block_index, carried_state):
        key_first = offset + block_index * sub_size

        def work(carried):
            top_score, totals, accum = carried
            block_rows = lax.dynamic_slice_in_dim(shard_part, block_index * sub_size, sub_size, 1)
            key_block = block_rows[:, :, :kv_cols].reshape(seq_count, sub_size, kv_local, head_dim)
            value_block = block_rows[:, :, kv_cols:].reshape(
                seq_count, sub_size, kv_local, head_dim
            )
            key_gates = lax.dynamic_slice_in_dim(forget_cache, key_first, sub_size, 2)
            key_gates = key_gates.reshape(seq_count, kv_local, head_group, 1, sub_size)
            scores = (
                jnp.einsum(
                    "bhqd,bkhd->bhqk", queries, key_block, preferred_element_type=jnp.float32
                )
                * scaling
            )
            scores = (
                scores.reshape(seq_count, kv_local, head_group, seq_span, sub_size)
                + own_gates
                - key_gates
            )
            scores = scores.reshape(seq_count, kv_local, head_group * seq_span, sub_size)
            visible = (
                query_pos[:, None] >= (key_first + jnp.arange(sub_size, dtype=jnp.int32))[None, :]
            )
            scores = jnp.where(visible, scores, -jnp.inf)
            new_top = jnp.maximum(top_score, jnp.max(scores, axis=-1))
            safe_top = jnp.where(jnp.isfinite(new_top), new_top, 0.0)
            weights = jnp.exp(scores - safe_top[..., None])
            fading = jnp.exp(top_score - safe_top)
            totals = totals * fading + jnp.sum(weights, axis=-1)
            accum = accum * fading[..., None] + jnp.einsum(
                "bhqk,bkhd->bhqd",
                weights.astype(jnp.bfloat16),
                value_block,
                preferred_element_type=jnp.float32,
            )
            return (new_top, totals, accum)

        return lax.cond(
            key_first < my_first + seq_span, work, lambda carried: carried, carried_state
        )

    _, totals, accum = lax.fori_loop(0, length // sub_size, one_step, start_state)
    attended = (accum / totals[..., None]).reshape(
        seq_count, kv_local, head_group, seq_span, head_dim
    )
    attended = attended.transpose(0, 3, 1, 2, 4).reshape(row_count, att_local, head_dim)
    att_normed = rms_scale(attended, attn_out_gain.reshape(att_local, head_dim)).astype(
        jnp.bfloat16
    )
    att_normed = att_normed.reshape(row_count, att_local * head_dim)
    rec_in = rec_in_sum.astype(jnp.bfloat16).reshape(seq_count, seq_span, channels)
    before = from_behind(rec_in[:, seq_span - (CONV_TAPS - 1) :, :], "sp", 1)
    extended = jnp.concatenate([before, rec_in], axis=1)
    conv = jnp.zeros((seq_count, seq_span, channels), jnp.float32)
    for tap in range(CONV_TAPS):
        conv = conv + extended[:, tap : tap + seq_span].astype(jnp.float32) * conv_weight[
            tap
        ].astype(jnp.float32)
    conv = conv.astype(jnp.bfloat16)
    blocks_local = decay_gate_weight.shape[0]
    grouped = conv.reshape(seq_count, seq_span, blocks_local, LRU_BLOCK)
    gate_decay = jnp.einsum(
        "bsnd,nde->bsne", grouped, decay_gate_weight, preferred_element_type=jnp.float32
    ).reshape(seq_count, seq_span, channels)
    gate_input = jnp.einsum(
        "bsnd,nde->bsne", grouped, input_gate_weight, preferred_element_type=jnp.float32
    ).reshape(seq_count, seq_span, channels)
    log_decay = (
        -lru_const * jax.nn.sigmoid(gate_decay) * jax.nn.softplus(-decay_param) + decay_extra
    )
    drive = (
        jnp.sqrt(-jnp.expm1(2.0 * log_decay))
        * jax.nn.sigmoid(gate_input)
        * conv.astype(jnp.float32)
    )
    cum_decay, local_state = lax.associative_scan(merge_state, (jnp.exp(log_decay), drive), axis=1)
    every_decay, every_state = (
        lax.all_gather(cum_decay[:, seq_span - 1][None], "sp", axis=0, tiled=True),
        lax.all_gather(local_state[:, seq_span - 1][None], "sp", axis=0, tiled=True),
    )
    _, prefix_state = lax.associative_scan(merge_state, (every_decay, every_state), axis=0)
    position = lax.axis_index("sp")
    earlier_state = lax.dynamic_index_in_dim(
        prefix_state, jnp.maximum(position - 1, 0), 0, keepdims=False
    )
    entering = jnp.where(position > 0, earlier_state, 0.0)
    state = local_state + cum_decay * entering[:, None, :]
    gated = state * jax.nn.gelu(gate_proj.reshape(seq_count, seq_span, channels))
    rec_normed = rms_scale(
        gated.reshape(row_count, blocks_local, LRU_BLOCK),
        rec_out_gain.reshape(blocks_local, LRU_BLOCK),
    ).astype(jnp.bfloat16)
    rec_normed = rec_normed.reshape(row_count, channels)
    out_cols = D // lax.axis_size("tp")
    pieces = row_count * lax.axis_size("tp") // row_count
    terms = jnp.dot(att_normed, out_att_weight, preferred_element_type=jnp.float32) + jnp.dot(
        rec_normed, out_rec_weight, preferred_element_type=jnp.float32
    )
    mixed_cols = lax.psum_scatter(
        terms.reshape(row_count, pieces, out_cols)
        .transpose(1, 0, 2)
        .reshape(pieces * row_count, out_cols)
        .astype(jnp.bfloat16),
        "tp",
        scatter_dimension=0,
        tiled=True,
    )
    return mixed_cols.reshape(seq_count, seq_span, out_cols)


BF16 = jnp.bfloat16
F32 = jnp.float32
HALO = 16
STATE_ROWS = 32
KERNEL_VMEM = 10 << 20


def ring_positions(count):
    return list(range(0, count, 2)) + list(range(count - 1, 0, -2))


def arrivals(place, count):
    at = jnp.where(place % 2 == 0, place // 2, count - 1 - place // 2)

    def member(position):
        position = (position + count) % count
        return jnp.where(position < count // 2, 2 * position, 2 * (count - 1 - position) + 1)

    found = [place]
    for step in range(1, count // 2):
        found += [member(at - step), member(at + step)]
    return found + [member(at + count // 2)]


class Ring:
    def __init__(self, own, count, last_forward):
        order = ring_positions(count)
        self.count = count
        self.forward = [(order[at], order[(at + 1) % count]) for at in range(count)]
        self.backward = [(target, source) for source, target in self.forward]
        self.last_forward = last_forward
        self.blocks = [own]
        self.ahead = own
        self.behind = own

    def step(self, number):
        last = number == self.count // 2
        if not last or self.last_forward:
            self.ahead = lax.ppermute(self.ahead, "sp", self.forward)
            self.blocks.append(self.ahead)
        if not last or not self.last_forward:
            self.behind = lax.ppermute(self.behind, "sp", self.backward)
            self.blocks.append(self.behind)


def vmem():
    return pl.BlockSpec(memory_space=pltpu.VMEM)


def call(kernel, outs, operands, scratch=()):
    single = not isinstance(outs, (list, tuple))
    return pl.pallas_call(
        kernel,
        out_shape=outs if single else tuple(outs),
        in_specs=[vmem()] * len(operands),
        out_specs=vmem() if single else tuple(vmem() for _ in outs),
        scratch_shapes=list(scratch),
        compiler_params=pltpu.CompilerParams(vmem_limit_bytes=KERNEL_VMEM),
    )(*operands)


def pack_kernel(key_ref, value_ref, rec_ref, out_ref):
    at = 0
    for part_ref in (key_ref, value_ref):
        size = part_ref.shape[0]
        out_ref[:, at : at + size] = part_ref[...].astype(F32).T.astype(BF16)
        at += size
    out_ref[:, at:] = rec_ref[...]


def pack_out_kernel(att_ref, rec_ref, *out_refs):
    place = lax.axis_index("tp")
    rows = att_ref.shape[0]
    for member, out_ref in enumerate(out_refs):
        width = out_ref.shape[1]
        columns = pl.ds(pl.multiple_of((place ^ member) * width, width), width)
        out_ref[:rows, :] = att_ref[:, columns]
        out_ref[rows:, :] = rec_ref[:, columns]


def block_diagonal(weight_ref):
    blocks, size, _ = weight_ref.shape
    tall = weight_ref[...].reshape(blocks * size, size)
    tiled = jnp.concatenate([tall] * blocks, axis=1)
    row = lax.broadcasted_iota(jnp.int32, tiled.shape, 0) // size
    column = lax.broadcasted_iota(jnp.int32, tiled.shape, 1) // size
    return jnp.where(row == column, tiled, jnp.zeros_like(tiled))


def norm_kernel(rows_ref, halo_ref, gain_ref, decay_ref, input_ref, out_ref, gates_ref):
    slices, _, width = out_ref.shape
    seq_count, span, _ = rows_ref.shape
    gain = gain_ref[...]
    kept = jnp.where(lax.axis_index("sp") > 0, 1.0, 0.0)
    for seq in range(seq_count):
        first = seq * (HALO + span)
        tail = halo_ref[seq].astype(F32) * kept
        tail = jnp.concatenate([jnp.zeros_like(tail), tail], axis=0)
        body_rows = rows_ref[seq].astype(F32)
        for values, at, size in ((tail, first, HALO), (body_rows, first + HALO, span)):
            normed = rms_scale(values, gain).astype(BF16)
            for part in range(slices):
                out_ref[part, at : at + size, :] = normed[:, part * width : (part + 1) * width]
    channels = gates_ref.shape[0]
    gates_ref[:, :channels] = block_diagonal(decay_ref)
    gates_ref[:, channels:] = block_diagonal(input_ref)


def softplus(value):
    small = jnp.exp(-jnp.abs(value))
    series = jnp.full_like(small, 1.0 / 7)
    for term in range(6, 0, -1):
        series = 1.0 / term - small * series
    return jnp.maximum(value, 0.0) + jnp.where(
        small < 0.05, small * series, jnp.log(1.0 + small)
    )


def gathered_dot(normed_ref, weight_refs, count, first=0, total=None):
    found = arrivals(lax.axis_index("sp"), count)[first:]
    for index, weight_ref in zip(found, weight_refs):
        term = jnp.dot(normed_ref[index], weight_ref[...], preferred_element_type=F32)
        total = term if total is None else total + term
    return total


def part_kernel(count, normed_ref, *refs):
    refs[-1][...] = gathered_dot(normed_ref, refs[:-1], count)


def minus_expm1(value, exp_value):
    series = jnp.full_like(value, 1.0)
    for term in range(9, 1, -1):
        series = 1.0 + value * (1.0 / term) * series
    return jnp.where(value > -0.5, -value * series, 1.0 - exp_value)


def shifted_down(value, steps, fill):
    moved = pltpu.roll(value, steps, 0)
    row = lax.broadcasted_iota(jnp.int32, value.shape, 0)
    return jnp.where(row >= steps, moved, fill)


def recurrence_kernel(count, head_dim, *refs):
    (
        normed_ref,
        part_ref,
        last_ref,
        key_gain_ref,
        taps_ref,
        gates_ref,
        decay_param_ref,
        extra_ref,
        message_ref,
        state_ref,
        decay_ref,
        rec_ref,
        ends_ref,
    ) = refs
    seq_count, span, channels = extra_ref.shape
    kv_width = 2 * head_dim
    sums = gathered_dot(normed_ref, [last_ref], count, count - 1, part_ref[...])
    rec_ref[...] = sums[:, kv_width:].astype(BF16).astype(F32)
    rate = softplus(-decay_param_ref[...])
    taps = taps_ref[...].astype(F32)
    key_gain = jnp.concatenate([key_gain_ref[...]] * 2, axis=1)
    lane = lax.broadcasted_iota(jnp.int32, (span, kv_width), 1)
    ends_ref[...] = jnp.zeros_like(ends_ref)
    halves = channels // kv_width
    for seq in range(seq_count):
        first = seq * (HALO + span)
        rows = pl.ds(seq * span, span)
        kv = sums[first + HALO : first + HALO + span, :kv_width]
        key = jnp.where(lane < head_dim, kv, 0.0)
        mean = jnp.sum(key * key, axis=-1, keepdims=True) * (1.0 / head_dim)
        scaled = kv * lax.rsqrt(mean + norm_eps) * key_gain
        message_ref[rows, :] = jnp.where(lane < head_dim, scaled, kv).astype(BF16)
        conv = jnp.zeros((span, channels), F32)
        for tap in range(CONV_TAPS):
            at = first + HALO - (CONV_TAPS - 1) + tap
            conv = conv + rec_ref[at : at + span, :] * taps[tap : tap + 1, :]
        conv = conv.astype(BF16)
        gated = jnp.dot(conv, gates_ref[...], preferred_element_type=F32)
        gate_decay, gate_input = gated[:, :channels], gated[:, channels:]
        log_decay = -lru_const * jax.nn.sigmoid(gate_decay) * rate + extra_ref[seq]
        decay = jnp.exp(log_decay)
        state = (
            jnp.sqrt(minus_expm1(2.0 * log_decay, decay * decay))
            * jax.nn.sigmoid(gate_input)
            * conv.astype(F32)
        )
        steps = 1
        while steps < span:
            state = state + decay * shifted_down(state, steps, 0.0)
            decay = decay * shifted_down(decay, steps, 1.0)
            steps *= 2
        state_ref[rows, :] = state
        decay_ref[rows, :] = decay
        for half in range(halves):
            lanes = slice(half * kv_width, (half + 1) * kv_width)
            at = seq * halves + half
            ends_ref[at : at + 1, :] = decay[span - 1 : span, lanes]
            at += seq_count * halves
            ends_ref[at : at + 1, :] = state[span - 1 : span, lanes]
    ends = ends_ref[...]
    high = ends.astype(BF16)
    left = ends - high.astype(F32)
    middle = left.astype(BF16)
    low = (left - middle.astype(F32)).astype(BF16)
    base = seq_count * span
    message_ref[base : base + 16, :] = jnp.concatenate([high, middle], axis=0)
    message_ref[base + 16 : base + 32, :] = jnp.concatenate([low, jnp.zeros_like(low)], axis=0)


def query_kernel(count, head_dim, seq_count, normed_ref, *refs):
    query_gain_ref, query_ref = refs[-2:]
    width = query_ref.shape[2]
    span = query_ref.shape[1]
    heads = query_ref.shape[0] // seq_count
    gain = jnp.concatenate([query_gain_ref[...]] * 2, axis=1)
    sums = gathered_dot(normed_ref, refs[:-2], count)
    lane = lax.broadcasted_iota(jnp.int32, (span, width), 1)
    scaling = head_dim ** (-0.5)
    for seq in range(seq_count):
        first = seq * (HALO + span) + HALO
        rows = sums[first : first + span]
        for head in range(heads):
            pair = rows[:, head // 2 * width : (head // 2 + 1) * width]
            if head % 2:
                pair = pltpu.roll(pair, head_dim, 1)
            own = jnp.where(lane < head_dim, pair, 0.0)
            mean = jnp.sum(own * own, axis=-1, keepdims=True) * (1.0 / head_dim)
            scaled = (own * lax.rsqrt(mean + norm_eps) * gain).astype(BF16)
            query_ref[seq * heads + head] = scaled * jnp.asarray(scaling, BF16)


def entering_kernel(count, group, *refs):
    place = lax.axis_index("sp")
    message_refs = refs[:count]
    (
        state_ref,
        decay_ref,
        normed_ref,
        part_ref,
        last_ref,
        gain_ref,
        out_ref,
        ends_ref,
    ) = refs[count:]
    gate = gathered_dot(normed_ref, [last_ref], count, count - 1, part_ref[...])
    rows, channels = state_ref.shape
    width = ends_ref.shape[2]
    halves = channels // width
    seq_count = ends_ref.shape[1] // (2 * halves)
    span = rows // seq_count
    for index, message_ref in zip(arrivals(place, count), message_refs):
        parts = message_ref[rows:, :].astype(F32)
        ends_ref[index] = parts[0:8] + parts[8:16] + parts[16:24]
    half_rows = seq_count * halves
    entering = jnp.zeros((half_rows, width), F32)
    for earlier in range(count - 1):
        ends = ends_ref[earlier]
        merged = ends[:half_rows] * entering + ends[half_rows:]
        entering = jnp.where(earlier < place, merged, entering)
    lane = lax.broadcasted_iota(jnp.int32, (span, width), 1)
    for seq in range(seq_count):
        for half in range(halves):
            lanes = slice(half * width, (half + 1) * width)
            at = seq * halves + half
            part = pl.ds(seq * span, span)
            first = seq * (HALO + span) + HALO
            state = state_ref[part, lanes] + decay_ref[part, lanes] * entering[at : at + 1, :]
            gated = state * jax.nn.gelu(gate[first : first + span, lanes])
            square = gated * gated
            total = jnp.sum(square, axis=-1, keepdims=True)
            low = jnp.sum(jnp.where(lane < group, square, 0.0), axis=-1, keepdims=True)
            mean = jnp.where(lane < group, low, total - low) * (1.0 / group)
            out_ref[part, lanes] = (
                gated * lax.rsqrt(mean + norm_eps) * gain_ref[:, lanes]
            ).astype(BF16)


def attention_kernel(count, head_dim, *refs):
    query_ref = refs[0]
    message_refs = refs[1 : 1 + count]
    gate_ref, gain_ref, out_ref, score_ref = refs[1 + count :]
    span, width = query_ref.shape[1:]
    rows = out_ref.shape[0]
    seq_count = rows // span
    heads = query_ref.shape[0] // seq_count
    place = lax.axis_index("sp")
    found = arrivals(place, count)
    ahead = lax.broadcasted_iota(jnp.int32, (span, span), 1) - lax.broadcasted_iota(
        jnp.int32, (span, span), 0
    )
    lane = lax.broadcasted_iota(jnp.int32, (span, width), 1)
    for seq in range(seq_count):
        keys = pl.ds(seq * span, span)
        queries = query_ref[seq * heads : (seq + 1) * heads].reshape(heads * span, width)
        top = [None] * heads
        own = gate_ref[seq, :, pl.ds(pl.multiple_of(place * span, span), span)]
        own = jnp.concatenate([own, jnp.zeros((span - heads, span), F32)], axis=0).T
        for at, block in enumerate(found):
            scores = lax.dot_general(
                queries,
                message_refs[at][keys, :],
                (((1,), (1,)), ((), ())),
                preferred_element_type=F32,
            )
            hidden = ahead > (place - block) * span
            gates = gate_ref[seq, :, pl.ds(pl.multiple_of(block * span, span), span)]
            for head in range(heads):
                score = scores[head * span : (head + 1) * span]
                score = score + own[:, head : head + 1] - gates[head : head + 1, :]
                score = jnp.where(hidden, -jnp.inf, score)
                score_ref[at, head * span : (head + 1) * span, :] = score
                top[head] = score if at == 0 else jnp.maximum(top[head], score)
        top = [jnp.max(part, axis=-1, keepdims=True) for part in top]
        totals = [None] * heads
        weighted = None
        for at in range(count):
            weights = []
            for head in range(heads):
                part = jnp.exp(score_ref[at, head * span : (head + 1) * span, :] - top[head])
                totals[head] = part if at == 0 else totals[head] + part
                weights.append(part.astype(BF16))
            term = jnp.dot(
                jnp.concatenate(weights, axis=0),
                message_refs[at][keys, :],
                preferred_element_type=F32,
            )
            weighted = term if at == 0 else weighted + term
        outs = []
        for head in range(heads):
            total = jnp.sum(totals[head], axis=-1, keepdims=True)
            attended = weighted[head * span : (head + 1) * span] / total
            attended = jnp.where(lane >= head_dim, attended, 0.0)
            mean = jnp.sum(attended * attended, axis=-1, keepdims=True) * (1.0 / head_dim)
            outs.append(attended * lax.rsqrt(mean + norm_eps))
        for pair in range(heads // 2):
            lanes = slice(pair * width, (pair + 1) * width)
            joined = jnp.where(
                lane < head_dim, pltpu.roll(outs[2 * pair], head_dim, 1), outs[2 * pair + 1]
            )
            out_ref[keys, lanes] = (joined * gain_ref[:, lanes]).astype(BF16)


def output_kernel(uses, has_base, *refs):
    out_ref = refs[-1]
    total = refs[-2][...] if has_base else None
    for left, right, half in uses:
        rows = refs[left].shape[1]
        term = jnp.dot(
            refs[left][...],
            refs[right][half * rows : (half + 1) * rows, :],
            preferred_element_type=F32,
        )
        total = term if total is None else total + term
    out_ref[...] = total.astype(out_ref.dtype)


def tp_spread(value, count):
    bits = [1 << at for at in range(count.bit_length() - 1)]
    found = {0: value}
    for bit in reversed(bits):
        pairs = [(source, source ^ bit) for source in range(count)]
        for member in sorted(found):
            found[member ^ bit] = lax.ppermute(found[member], "tp", pairs)
    return [found[member] for member in range(count)]


def ring_body(
    inputs,
    norm_gain,
    query_weight,
    key_weight,
    value_weight,
    query_gain,
    key_gain,
    forget_cache,
    rec_in_weight,
    rec_gate_weight,
    conv_weight,
    decay_gate_weight,
    input_gate_weight,
    decay_param,
    decay_extra,
    attn_out_gain,
    rec_out_gain,
    out_att_weight,
    out_rec_weight,
):
    count = lax.axis_size("sp")
    tp_count = lax.axis_size("tp")
    seq_count, span, model_width = inputs.shape
    rows = seq_count * span
    head_dim = query_gain.shape[0]
    width = 2 * head_dim
    att_width = query_weight.shape[1]
    heads = att_width // head_dim
    channels = rec_in_weight.shape[1]
    ext_rows = seq_count * (HALO + span)
    out_cols = model_width // tp_count
    query_ring = Ring(query_weight, count, False)
    query_ring.step(1)
    first_chunk = call(
        pack_kernel,
        jax.ShapeDtypeStruct((rec_in_weight.shape[0], width + channels), BF16),
        [key_weight.T, value_weight.T, rec_in_weight],
    )
    first_ring = Ring(first_chunk, count, True)
    first_ring.step(1)
    shift = [(member, (member + 1) % count) for member in range(count)]
    halo = lax.ppermute(inputs[:, span - HALO // 2 :, :], "sp", shift)

    normed, gate_weights = call(
        norm_kernel,
        [
            jax.ShapeDtypeStruct((count, ext_rows, model_width // count), BF16),
            jax.ShapeDtypeStruct((channels, 2 * channels), BF16),
        ],
        [inputs, halo, norm_gain.reshape(1, model_width), decay_gate_weight, input_gate_weight],
    )
    out_weight = call(
        pack_out_kernel,
        [jax.ShapeDtypeStruct((att_width + channels, out_cols), BF16) for _ in range(tp_count)],
        [out_att_weight, out_rec_weight],
    )
    out_weight = [out_weight[0]] + [
        lax.ppermute(
            out_weight[member], "tp", [(source, source ^ member) for source in range(tp_count)]
        )
        for member in range(1, tp_count)
    ]

    for number in range(2, count // 2 + 1):
        first_ring.step(number)
        query_ring.step(number)
    gate_ring = Ring(rec_gate_weight, count, False)
    for number in range(1, count // 2 + 1):
        gate_ring.step(number)

    def part_of(ring):
        columns = ring.blocks[0].shape[1]
        return call(
            functools.partial(part_kernel, count),
            jax.ShapeDtypeStruct((ext_rows, columns), F32),
            [normed, *ring.blocks[:-1]],
        )

    message, local_state, cum_decay = call(
        functools.partial(recurrence_kernel, count, head_dim),
        [
            jax.ShapeDtypeStruct((rows + STATE_ROWS, width), BF16),
            jax.ShapeDtypeStruct((rows, channels), F32),
            jax.ShapeDtypeStruct((rows, channels), F32),
        ],
        [
            normed,
            part_of(first_ring),
            first_ring.blocks[-1],
            key_gain.reshape(1, head_dim),
            conv_weight,
            gate_weights,
            decay_param.reshape(1, channels),
            decay_extra,
        ],
        scratch=[pltpu.VMEM((ext_rows, channels), F32), pltpu.VMEM((8, width), F32)],
    )
    message_ring = Ring(message, count, True)
    for number in range(1, count // 2 + 1):
        message_ring.step(number)

    queries = call(
        functools.partial(query_kernel, count, head_dim, seq_count),
        jax.ShapeDtypeStruct((seq_count * heads, span, width), BF16),
        [normed, *query_ring.blocks, query_gain.reshape(1, head_dim)],
    )
    messages = message_ring.blocks
    rec_normed = call(
        functools.partial(entering_kernel, count, LRU_BLOCK),
        jax.ShapeDtypeStruct((rows, channels), BF16),
        [
            *messages,
            local_state,
            cum_decay,
            normed,
            part_of(gate_ring),
            gate_ring.blocks[-1],
            rec_out_gain.reshape(1, channels),
        ],
        scratch=[pltpu.VMEM((count, 8, width), F32)],
    )
    att_normed = call(
        functools.partial(attention_kernel, count, head_dim),
        jax.ShapeDtypeStruct((rows, att_width), BF16),
        [queries, *messages, forget_cache, attn_out_gain.reshape(1, att_width)],
        scratch=[pltpu.VMEM((count, heads * span, span), F32)],
    )

    def project(rec_members, att_members, base, kind):
        operands, uses = [], []
        weights = sorted({*rec_members, *att_members})
        for parts, half, members in ((rec_parts, 1, rec_members), (att_parts, 0, att_members)):
            for member in members:
                uses.append((len(operands), -1 - member, half))
                operands.append(parts[member])
        at_weight = {member: len(operands) + at for at, member in enumerate(weights)}
        uses = [(left, at_weight[-1 - right], half) for left, right, half in uses]
        operands += [out_weight[member] for member in weights]
        if base is not None:
            operands.append(base)
        return call(
            functools.partial(output_kernel, tuple(uses), base is not None),
            jax.ShapeDtypeStruct((rows, out_cols), kind),
            operands,
        )

    rec_parts = tp_spread(rec_normed, tp_count)
    att_parts = tp_spread(att_normed, tp_count)
    near, far = range(tp_count // 2), range(tp_count // 2, tp_count)
    base = project(range(tp_count), near, None, F32)
    mixed = project((), far, base, BF16)
    return mixed.reshape(seq_count, span, out_cols)


def fits(count, tp_count):
    return 4 <= count <= 16 and count % 2 == 0 and tp_count in (2, 4)


def layer(*arrays):
    inputs, query_weight, key_weight = arrays[0], arrays[2], arrays[3]
    head_dim, rec_in_weight = arrays[5].shape[0], arrays[8]
    count, tp_count = lax.axis_size("sp"), lax.axis_size("tp")
    whole_blocks = (
        inputs.shape[0] * rec_in_weight.shape[1] == 8 * head_dim
        and inputs.shape[1] == 2 * head_dim
        and key_weight.shape[1] == head_dim
        and query_weight.shape[1] == rec_in_weight.shape[1]
        and inputs.shape[2] % (128 * count) == 0
    )
    return (ring_body if fits(count, tp_count) and whole_blocks else body)(*arrays)


def solution(mesh):
    return jax.shard_map(
        layer,
        mesh=mesh,
        in_specs=(
            P(None, "sp", None),
            P(),
            P("sp", "tp"),
            P("sp", "tp"),
            P("sp", "tp"),
            P(),
            P(),
            P(None, "tp", None),
            P("sp", "tp"),
            P("sp", "tp"),
            P(None, "tp"),
            P("tp", None, None),
            P("tp", None, None),
            P("tp"),
            P(None, "sp", "tp"),
            P("tp"),
            P("tp"),
            P("tp", None),
            P("tp", None),
        ),
        out_specs=P(None, "sp", "tp"),
        check_vma=False,
    )
```

profile of v0, /device:TPU:0, one launch (start us, length us, event | category | flops | bytes accessed | tf_op | source)
XLA Modules:
  0.0 84.0 jit_solution(7608279645187082613)
XLA Ops:
  2.6 3.1 %collective-permute-start.8 = (bf16[256,384]{1,0:T(8,128)(2,1)S(1)}, bf16[256,384]{1,0:T(8,128)(2,1)S(1)}, u32[]{:S(2)}, u32[]{:S(2)}) collective-permute-start(bf16[256,384]{1,0:T(8,128)(2,1)S(1)} %shard_map.183.refs_0_), channel_id=1, source_target_pairs={{0,8},{8,16},{16,24},{24,28},{28,20},{20,12},{12,4},{4,0},{1,9},{9... | collective-permute-start | bytes 589832 | tf_op jit(solution)/shard_map/ppermute | solution.py:275
  5.7 4.8 %collective-permute-done.8.refs_1_ = bf16[256,384]{1,0:T(8,128)(2,1)S(1)} collective-permute-done((bf16[256,384]{1,0:T(8,128)(2,1)S(1)}, bf16[256,384]{1,0:T(8,128)(2,1)S(1)}, u32[]{:S(2)}, u32[]{:S(2)}) %collective-permute-start.8) | collective-permute-done | bytes 196640 | tf_op jit(solution)/shard_map/ppermute | solution.py:275
  10.6 1.8 %collective-permute-start.10 = (bf16[256,384]{1,0:T(8,128)(2,1)S(1)}, bf16[256,384]{1,0:T(8,128)(2,1)S(1)}, u32[]{:S(2)}, u32[]{:S(2)}) collective-permute-start(bf16[256,384]{1,0:T(8,128)(2,1)S(1)} %collective-permute-done.8.refs_1_), channel_id=1, source_target_pairs={{0,8},{8,16},{16,24},{24,28},{28,20},{20,12},{12,4},{4,0},{1,9},{9... | collective-permute-start | bytes 589832 | tf_op jit(solution)/shard_map/ppermute | solution.py:275
  12.6 1.8 %collective-permute-start.26 = (bf16[256,256]{1,0:T(8,128)(2,1)}, bf16[256,256]{1,0:T(8,128)(2,1)S(1)}, u32[]{:S(2)}, u32[]{:S(2)}) collective-permute-start(bf16[256,256]{1,0:T(8,128)(2,1)} %refs_0_.3), channel_id=1, source_target_pairs={{0,8},{8,16},{16,24},{24,28},{28,20},{20,12},{12,4},{4,0},{1,9},{9... | collective-permute-start | bytes 393224 | tf_op jit(solution)/shard_map/ppermute | solution.py:275
  15.5 8.3 %collective-permute-done.halo_ref = bf16[2,8,2048]{2,1,0:T(8,128)(2,1)S(1)} collective-permute-done((bf16[2,8,2048]{2,1,0:T(8,128)(2,1)S(1)}, bf16[2,8,2048]{2,1,0:T(8,128)(2,1)S(1)}, u32[]{:S(2)}, u32[]{:S(2)}) %collective-permute-start) | collective-permute-done | bytes 65568 | tf_op jit(solution)/shard_map/ppermute | solution.py:650
  23.8 2.0 %collective-permute-start.1 = (bf16[256,256]{1,0:T(8,128)(2,1)}, bf16[256,256]{1,0:T(8,128)(2,1)S(1)}, u32[]{:S(2)}, u32[]{:S(2)}) collective-permute-start(bf16[256,256]{1,0:T(8,128)(2,1)} %refs_0_.2), channel_id=1, source_target_pairs={{0,8},{8,16},{16,24},{24,28},{28,20},{20,12},{12,4},{4,0},{1,9},{9... | collective-permute-start | bytes 393224 | tf_op jit(solution)/shard_map/ppermute | solution.py:275
  25.9 2.0 %collective-permute-start.12 = (bf16[256,384]{1,0:T(8,128)(2,1)S(1)}, bf16[256,384]{1,0:T(8,128)(2,1)S(1)}, u32[]{:S(2)}, u32[]{:S(2)}) collective-permute-start(bf16[256,384]{1,0:T(8,128)(2,1)S(1)} %collective-permute-done.10.refs_3_), channel_id=1, source_target_pairs={{0,8},{8,16},{16,24},{24,28},{28,20},{20,12},{12,4},{4,0},{1,9},{9... | collective-permute-start | bytes 589832 | tf_op jit(solution)/shard_map/ppermute | solution.py:275
  27.9 2.5 %collective-permute-done.2.refs_2_ = bf16[256,256]{1,0:T(8,128)(2,1)S(1)} collective-permute-done((bf16[256,256]{1,0:T(8,128)(2,1)}, bf16[256,256]{1,0:T(8,128)(2,1)S(1)}, u32[]{:S(2)}, u32[]{:S(2)}) %collective-permute-start.2) | collective-permute-done | bytes 131104 | tf_op jit(solution)/shard_map/ppermute | solution.py:278
  30.4 2.0 %collective-permute-start.4 = (bf16[256,256]{1,0:T(8,128)(2,1)S(1)}, bf16[256,256]{1,0:T(8,128)(2,1)S(1)}, u32[]{:S(2)}, u32[]{:S(2)}) collective-permute-start(bf16[256,256]{1,0:T(8,128)(2,1)S(1)} %collective-permute-done.2.refs_2_), channel_id=1, source_target_pairs={{8,0},{16,8},{24,16},{28,24},{20,28},{12,20},{4,12},{0,4},{9,1},{1... | collective-permute-start | bytes 393224 | tf_op jit(solution)/shard_map/ppermute | solution.py:278
  33.2 4.2 %collective-permute-done.11.refs_4_ = bf16[256,384]{1,0:T(8,128)(2,1)S(1)} collective-permute-done((bf16[256,384]{1,0:T(8,128)(2,1)S(1)}, bf16[256,384]{1,0:T(8,128)(2,1)S(1)}, u32[]{:S(2)}, u32[]{:S(2)}) %collective-permute-start.11) | collective-permute-done | bytes 196640 | tf_op jit(solution)/shard_map/ppermute | solution.py:278
  37.4 2.1 %collective-permute-start.14 = (bf16[256,384]{1,0:T(8,128)(2,1)S(1)}, bf16[256,384]{1,0:T(8,128)(2,1)S(1)}, u32[]{:S(2)}, u32[]{:S(2)}) collective-permute-start(bf16[256,384]{1,0:T(8,128)(2,1)S(1)} %collective-permute-done.12.refs_5_), channel_id=1, source_target_pairs={{0,8},{8,16},{16,24},{24,28},{28,20},{20,12},{12,4},{4,0},{1,9},{9... | collective-permute-start | bytes 589832 | tf_op jit(solution)/shard_map/ppermute | solution.py:275
  42.2 3.3 %collective-permute-done.31.refs_6_ = bf16[256,256]{1,0:T(8,128)(2,1)S(1)} collective-permute-done((bf16[256,256]{1,0:T(8,128)(2,1)S(1)}, bf16[256,256]{1,0:T(8,128)(2,1)S(1)}, u32[]{:S(2)}, u32[]{:S(2)}) %collective-permute-start.31) | collective-permute-done | bytes 131104 | tf_op jit(solution)/shard_map/ppermute | solution.py:278
  48.3 1.6 %collective-permute-start.24 = (bf16[512,512]{1,0:T(8,128)(2,1)S(1)}, bf16[512,512]{1,0:T(8,128)(2,1)S(1)}, u32[]{:S(2)}, u32[]{:S(2)}) collective-permute-start(bf16[512,512]{1,0:T(8,128)(2,1)S(1)} %get-tuple-element.17), channel_id=1, source_target_pairs={{0,2},{1,3},{2,0},{3,1},{4,6},{5,7},{6,4},{7,5},{8,10},{9,11},{10,... | collective-permute-start | bytes 1572872 | tf_op jit(solution)/shard_map/ppermute | solution.py:666
  49.8 1.8 %collective-permute-start.32 = (bf16[256,256]{1,0:T(8,128)(2,1)S(1)}, bf16[256,256]{1,0:T(8,128)(2,1)S(1)}, u32[]{:S(2)}, u32[]{:S(2)}) collective-permute-start(bf16[256,256]{1,0:T(8,128)(2,1)S(1)} %collective-permute-done.31.refs_6_), channel_id=1, source_target_pairs={{8,0},{16,8},{24,16},{28,24},{20,28},{12,20},{4,12},{0,4},{9,1},{1... | collective-permute-start | bytes 393224 | tf_op jit(solution)/shard_map/ppermute | solution.py:278
  54.8 1.8 %collective-permute-start.15 = (bf16[288,128]{1,0:T(8,128)(2,1)S(1)}, bf16[288,128]{1,0:T(8,128)(2,1)S(1)}, u32[]{:S(2)}, u32[]{:S(2)}) collective-permute-start(bf16[288,128]{1,0:T(8,128)(2,1)S(1)} %get-tuple-element.16.refs_1_.refs_0_), channel_id=1, source_target_pairs={{0,8},{8,16},{16,24},{24,28},{28,20},{20,12},{12,4},{4,0},{1,9},{9... | collective-permute-start | bytes 221192 | tf_op jit(solution)/shard_map/ppermute | solution.py:275
  57.7 1.7 %collective-permute-start.16 = (bf16[288,128]{1,0:T(8,128)(2,1)S(1)}, bf16[288,128]{1,0:T(8,128)(2,1)S(1)}, u32[]{:S(2)}, u32[]{:S(2)}) collective-permute-start(bf16[288,128]{1,0:T(8,128)(2,1)S(1)} %get-tuple-element.16.refs_1_.refs_0_), channel_id=1, source_target_pairs={{8,0},{16,8},{24,16},{28,24},{20,28},{12,20},{4,12},{0,4},{9,1},{1... | collective-permute-start | bytes 221192 | tf_op jit(solution)/shard_map/ppermute | solution.py:278
  59.4 1.6 %collective-permute-start.17 = (bf16[288,128]{1,0:T(8,128)(2,1)S(1)}, bf16[288,128]{1,0:T(8,128)(2,1)S(1)}, u32[]{:S(2)}, u32[]{:S(2)}) collective-permute-start(bf16[288,128]{1,0:T(8,128)(2,1)S(1)} %collective-permute-done.15.refs_2_.refs_1_), channel_id=1, source_target_pairs={{0,8},{8,16},{16,24},{24,28},{28,20},{20,12},{12,4},{4,0},{1,9},{9... | collective-permute-start | bytes 221192 | tf_op jit(solution)/shard_map/ppermute | solution.py:275
  62.1 1.7 %collective-permute-start.18 = (bf16[288,128]{1,0:T(8,128)(2,1)S(1)}, bf16[288,128]{1,0:T(8,128)(2,1)S(1)}, u32[]{:S(2)}, u32[]{:S(2)}) collective-permute-start(bf16[288,128]{1,0:T(8,128)(2,1)S(1)} %collective-permute-done.16.refs_3_.refs_2_), channel_id=1, source_target_pairs={{8,0},{16,8},{24,16},{28,24},{20,28},{12,20},{4,12},{0,4},{9,1},{1... | collective-permute-start | bytes 221192 | tf_op jit(solution)/shard_map/ppermute | solution.py:278
  63.8 1.6 %collective-permute-start.19 = (bf16[288,128]{1,0:T(8,128)(2,1)S(1)}, bf16[288,128]{1,0:T(8,128)(2,1)S(1)}, u32[]{:S(2)}, u32[]{:S(2)}) collective-permute-start(bf16[288,128]{1,0:T(8,128)(2,1)S(1)} %collective-permute-done.17.refs_4_.refs_3_), channel_id=1, source_target_pairs={{0,8},{8,16},{16,24},{24,28},{28,20},{20,12},{12,4},{4,0},{1,9},{9... | collective-permute-start | bytes 221192 | tf_op jit(solution)/shard_map/ppermute | solution.py:275
  66.4 1.7 %collective-permute-start.20 = (bf16[288,128]{1,0:T(8,128)(2,1)S(1)}, bf16[288,128]{1,0:T(8,128)(2,1)S(1)}, u32[]{:S(2)}, u32[]{:S(2)}) collective-permute-start(bf16[288,128]{1,0:T(8,128)(2,1)S(1)} %collective-permute-done.18.refs_5_.refs_4_), channel_id=1, source_target_pairs={{8,0},{16,8},{24,16},{28,24},{20,28},{12,20},{4,12},{0,4},{9,1},{1... | collective-permute-start | bytes 221192 | tf_op jit(solution)/shard_map/ppermute | solution.py:278
  68.1 1.6 %collective-permute-start.21 = (bf16[288,128]{1,0:T(8,128)(2,1)S(1)}, bf16[288,128]{1,0:T(8,128)(2,1)S(1)}, u32[]{:S(2)}, u32[]{:S(2)}) collective-permute-start(bf16[288,128]{1,0:T(8,128)(2,1)S(1)} %collective-permute-done.19.refs_6_.refs_5_), channel_id=1, source_target_pairs={{0,8},{8,16},{16,24},{24,28},{28,20},{20,12},{12,4},{4,0},{1,9},{9... | collective-permute-start | bytes 221192 | tf_op jit(solution)/shard_map/ppermute | solution.py:275
  70.2 1.3 %shard_map.182.refs_0_ = bf16[8,128,128]{2,1,0:T(8,128)(2,1)S(1)} custom-call(bf16[8,288,256]{2,1,0:T(8,128)(2,1)S(1)} %get-tuple-element.14.normed_ref.refs_0_.refs_10_, bf16[256,256]{1,0:T(8,128)(2,1)S(1)} %copy-done.6, bf16[256,256]{1,0:T(8,128)(2,1)S(1)} %collective-permute-done.1.refs_1_, bf16[256,256]{1,0:T(8,128)(2,1)S(1)} %collective-permute-done.2.refs_2_, ...), custom_call_target="tpu_custom_call" | custom-call | tf_op jit(solution)/shard_map/pallas_call | solution.py:288
  74.0 2.7 %shard_map.186.refs_4_ = bf16[256,256]{1,0:T(8,128)(2,1)S(1)} custom-call(bf16[8,128,128]{2,1,0:T(8,128)(2,1)S(1)} %shard_map.182.refs_0_, bf16[288,128]{1,0:T(8,128)(2,1)S(1)} %get-tuple-element.16.refs_1_.refs_0_, bf16[288,128]{1,0:T(8,128)(2,1)S(1)} %collective-permute-done.15.refs_2_.refs_1_, ...), custom_call_target="tpu_custom_call" | custom-call | tf_op jit(solution)/shard_map/pallas_call | solution.py:288
  79.3 2.4 %collective-permute-done.22.refs_0_ = bf16[256,256]{1,0:T(8,128)(2,1)S(1)} collective-permute-done((bf16[256,256]{1,0:T(8,128)(2,1)S(1)}, bf16[256,256]{1,0:T(8,128)(2,1)S(1)}, u32[]{:S(2)}, u32[]{:S(2)}) %collective-permute-start.22) | collective-permute-done | bytes 131104 | tf_op jit(solution)/shard_map/ppermute | solution.py:604
  (102 shorter events, 24.5 us)
Async XLA Ops:
  2.6 7.9 %collective-permute-start.8 = (bf16[256,384]{1,0:T(8,128)(2,1)S(1)}, bf16[256,384]{1,0:T(8,128)(2,1)S(1)}, u32[]{:S(2)}, u32[]{:S(2)}) collective-permute-start(bf16[256,384]{1,0:T(8,128)(2,1)S(1)} %shard_map.183.refs_0_), channel_id=1, source_target_pairs={{0,8},{8,16},{16,24},{24,28},{28,20},{20,12},{12,4},{4,0},{1,9},{9... | collective-permute-start | bytes 589832 | tf_op jit(solution)/shard_map/ppermute | solution.py:275
  5.7 20.1 %collective-permute-start.9 = (bf16[256,384]{1,0:T(8,128)(2,1)S(1)}, bf16[256,384]{1,0:T(8,128)(2,1)S(1)}, u32[]{:S(2)}, u32[]{:S(2)}) collective-permute-start(bf16[256,384]{1,0:T(8,128)(2,1)S(1)} %shard_map.183.refs_0_), channel_id=1, source_target_pairs={{8,0},{16,8},{24,16},{28,24},{20,28},{12,20},{4,12},{0,4},{9,1},{1... | collective-permute-start | bytes 589832 | tf_op jit(solution)/shard_map/ppermute | solution.py:278
  10.6 15.3 %collective-permute-start.10 = (bf16[256,384]{1,0:T(8,128)(2,1)S(1)}, bf16[256,384]{1,0:T(8,128)(2,1)S(1)}, u32[]{:S(2)}, u32[]{:S(2)}) collective-permute-start(bf16[256,384]{1,0:T(8,128)(2,1)S(1)} %collective-permute-done.8.refs_1_), channel_id=1, source_target_pairs={{0,8},{8,16},{16,24},{24,28},{28,20},{20,12},{12,4},{4,0},{1,9},{9... | collective-permute-start | bytes 589832 | tf_op jit(solution)/shard_map/ppermute | solution.py:275
  12.4 11.4 %collective-permute-start.27 = (bf16[256,256]{1,0:T(8,128)(2,1)}, bf16[256,256]{1,0:T(8,128)(2,1)S(1)}, u32[]{:S(2)}, u32[]{:S(2)}) collective-permute-start(bf16[256,256]{1,0:T(8,128)(2,1)} %refs_0_.3), channel_id=1, source_target_pairs={{8,0},{16,8},{24,16},{28,24},{20,28},{12,20},{4,12},{0,4},{9,1},{1... | collective-permute-start | bytes 393224 | tf_op jit(solution)/shard_map/ppermute | solution.py:278
  12.6 13.2 %collective-permute-start.26 = (bf16[256,256]{1,0:T(8,128)(2,1)}, bf16[256,256]{1,0:T(8,128)(2,1)S(1)}, u32[]{:S(2)}, u32[]{:S(2)}) collective-permute-start(bf16[256,256]{1,0:T(8,128)(2,1)} %refs_0_.3), channel_id=1, source_target_pairs={{0,8},{8,16},{16,24},{24,28},{28,20},{20,12},{12,4},{4,0},{1,9},{9... | collective-permute-start | bytes 393224 | tf_op jit(solution)/shard_map/ppermute | solution.py:275
  15.2 8.5 %collective-permute-start = (bf16[2,8,2048]{2,1,0:T(8,128)(2,1)S(1)}, bf16[2,8,2048]{2,1,0:T(8,128)(2,1)S(1)}, u32[]{:S(2)}, u32[]{:S(2)}) collective-permute-start(bf16[2,8,2048]{2,1,0:T(8,128)(2,1)S(1)} %slice.3), channel_id=1, source_target_pairs={{0,4},{4,8},{8,12},{12,16},{16,20},{20,24},{24,28},{28,0},{1,5},{5... | collective-permute-start | bytes 196616 | tf_op jit(solution)/shard_map/ppermute | solution.py:650
  23.8 6.6 %collective-permute-start.2 = (bf16[256,256]{1,0:T(8,128)(2,1)}, bf16[256,256]{1,0:T(8,128)(2,1)S(1)}, u32[]{:S(2)}, u32[]{:S(2)}) collective-permute-start(bf16[256,256]{1,0:T(8,128)(2,1)} %refs_0_.2), channel_id=1, source_target_pairs={{8,0},{16,8},{24,16},{28,24},{20,28},{12,20},{4,12},{0,4},{9,1},{1... | collective-permute-start | bytes 393224 | tf_op jit(solution)/shard_map/ppermute | solution.py:278
  23.8 6.6 %collective-permute-start.1 = (bf16[256,256]{1,0:T(8,128)(2,1)}, bf16[256,256]{1,0:T(8,128)(2,1)S(1)}, u32[]{:S(2)}, u32[]{:S(2)}) collective-permute-start(bf16[256,256]{1,0:T(8,128)(2,1)} %refs_0_.2), channel_id=1, source_target_pairs={{0,8},{8,16},{16,24},{24,28},{28,20},{20,12},{12,4},{4,0},{1,9},{9... | collective-permute-start | bytes 393224 | tf_op jit(solution)/shard_map/ppermute | solution.py:275
  25.8 7.4 %collective-permute-start.29 = (bf16[256,256]{1,0:T(8,128)(2,1)S(1)}, bf16[256,256]{1,0:T(8,128)(2,1)S(1)}, u32[]{:S(2)}, u32[]{:S(2)}) collective-permute-start(bf16[256,256]{1,0:T(8,128)(2,1)S(1)} %collective-permute-done.27.refs_2_), channel_id=1, source_target_pairs={{8,0},{16,8},{24,16},{28,24},{20,28},{12,20},{4,12},{0,4},{9,1},{1... | collective-permute-start | bytes 393224 | tf_op jit(solution)/shard_map/ppermute | solution.py:278
  25.8 11.6 %collective-permute-start.11 = (bf16[256,384]{1,0:T(8,128)(2,1)S(1)}, bf16[256,384]{1,0:T(8,128)(2,1)S(1)}, u32[]{:S(2)}, u32[]{:S(2)}) collective-permute-start(bf16[256,384]{1,0:T(8,128)(2,1)S(1)} %collective-permute-done.9.refs_2_), channel_id=1, source_target_pairs={{8,0},{16,8},{24,16},{28,24},{20,28},{12,20},{4,12},{0,4},{9,1},{1... | collective-permute-start | bytes 589832 | tf_op jit(solution)/shard_map/ppermute | solution.py:278
  25.9 11.5 %collective-permute-start.12 = (bf16[256,384]{1,0:T(8,128)(2,1)S(1)}, bf16[256,384]{1,0:T(8,128)(2,1)S(1)}, u32[]{:S(2)}, u32[]{:S(2)}) collective-permute-start(bf16[256,384]{1,0:T(8,128)(2,1)S(1)} %collective-permute-done.10.refs_3_), channel_id=1, source_target_pairs={{0,8},{8,16},{16,24},{24,28},{28,20},{20,12},{12,4},{4,0},{1,9},{9... | collective-permute-start | bytes 589832 | tf_op jit(solution)/shard_map/ppermute | solution.py:275
  30.3 7.0 %collective-permute-start.28 = (bf16[256,256]{1,0:T(8,128)(2,1)S(1)}, bf16[256,256]{1,0:T(8,128)(2,1)S(1)}, u32[]{:S(2)}, u32[]{:S(2)}) collective-permute-start(bf16[256,256]{1,0:T(8,128)(2,1)S(1)} %collective-permute-done.26.refs_1_), channel_id=1, source_target_pairs={{0,8},{8,16},{16,24},{24,28},{28,20},{20,12},{12,4},{4,0},{1,9},{9... | collective-permute-start | bytes 393224 | tf_op jit(solution)/shard_map/ppermute | solution.py:275
  30.4 9.8 %collective-permute-start.4 = (bf16[256,256]{1,0:T(8,128)(2,1)S(1)}, bf16[256,256]{1,0:T(8,128)(2,1)S(1)}, u32[]{:S(2)}, u32[]{:S(2)}) collective-permute-start(bf16[256,256]{1,0:T(8,128)(2,1)S(1)} %collective-permute-done.2.refs_2_), channel_id=1, source_target_pairs={{8,0},{16,8},{24,16},{28,24},{20,28},{12,20},{4,12},{0,4},{9,1},{1... | collective-permute-start | bytes 393224 | tf_op jit(solution)/shard_map/ppermute | solution.py:278
  33.2 8.3 %collective-permute-start.3 = (bf16[256,256]{1,0:T(8,128)(2,1)S(1)}, bf16[256,256]{1,0:T(8,128)(2,1)S(1)}, u32[]{:S(2)}, u32[]{:S(2)}) collective-permute-start(bf16[256,256]{1,0:T(8,128)(2,1)S(1)} %collective-permute-done.1.refs_1_), channel_id=1, source_target_pairs={{0,8},{8,16},{16,24},{24,28},{28,20},{20,12},{12,4},{4,0},{1,9},{9... | collective-permute-start | bytes 393224 | tf_op jit(solution)/shard_map/ppermute | solution.py:275
  37.4 14.3 %collective-permute-start.13 = (bf16[256,384]{1,0:T(8,128)(2,1)S(1)}, bf16[256,384]{1,0:T(8,128)(2,1)S(1)}, u32[]{:S(2)}, u32[]{:S(2)}) collective-permute-start(bf16[256,384]{1,0:T(8,128)(2,1)S(1)} %collective-permute-done.11.refs_4_), channel_id=1, source_target_pairs={{8,0},{16,8},{24,16},{28,24},{20,28},{12,20},{4,12},{0,4},{9,1},{1... | collective-permute-start | bytes 589832 | tf_op jit(solution)/shard_map/ppermute | solution.py:278
  37.4 8.1 %collective-permute-start.31 = (bf16[256,256]{1,0:T(8,128)(2,1)S(1)}, bf16[256,256]{1,0:T(8,128)(2,1)S(1)}, u32[]{:S(2)}, u32[]{:S(2)}) collective-permute-start(bf16[256,256]{1,0:T(8,128)(2,1)S(1)} %collective-permute-done.29.refs_4_), channel_id=1, source_target_pairs={{8,0},{16,8},{24,16},{28,24},{20,28},{12,20},{4,12},{0,4},{9,1},{1... | collective-permute-start | bytes 393224 | tf_op jit(solution)/shard_map/ppermute | solution.py:278
  37.4 14.3 %collective-permute-start.14 = (bf16[256,384]{1,0:T(8,128)(2,1)S(1)}, bf16[256,384]{1,0:T(8,128)(2,1)S(1)}, u32[]{:S(2)}, u32[]{:S(2)}) collective-permute-start(bf16[256,384]{1,0:T(8,128)(2,1)S(1)} %collective-permute-done.12.refs_5_), channel_id=1, source_target_pairs={{0,8},{8,16},{16,24},{24,28},{28,20},{20,12},{12,4},{4,0},{1,9},{9... | collective-permute-start | bytes 589832 | tf_op jit(solution)/shard_map/ppermute | solution.py:275
  40.2 8.1 %collective-permute-start.30 = (bf16[256,256]{1,0:T(8,128)(2,1)S(1)}, bf16[256,256]{1,0:T(8,128)(2,1)S(1)}, u32[]{:S(2)}, u32[]{:S(2)}) collective-permute-start(bf16[256,256]{1,0:T(8,128)(2,1)S(1)} %collective-permute-done.28.refs_3_), channel_id=1, source_target_pairs={{0,8},{8,16},{16,24},{24,28},{28,20},{20,12},{12,4},{4,0},{1,9},{9... | collective-permute-start | bytes 393224 | tf_op jit(solution)/shard_map/ppermute | solution.py:275
  41.4 8.4 %collective-permute-start.6 = (bf16[256,256]{1,0:T(8,128)(2,1)S(1)}, bf16[256,256]{1,0:T(8,128)(2,1)S(1)}, u32[]{:S(2)}, u32[]{:S(2)}) collective-permute-start(bf16[256,256]{1,0:T(8,128)(2,1)S(1)} %collective-permute-done.4.refs_4_), channel_id=1, source_target_pairs={{8,0},{16,8},{24,16},{28,24},{20,28},{12,20},{4,12},{0,4},{9,1},{1... | collective-permute-start | bytes 393224 | tf_op jit(solution)/shard_map/ppermute | solution.py:278
  45.5 9.3 %collective-permute-start.5 = (bf16[256,256]{1,0:T(8,128)(2,1)S(1)}, bf16[256,256]{1,0:T(8,128)(2,1)S(1)}, u32[]{:S(2)}, u32[]{:S(2)}) collective-permute-start(bf16[256,256]{1,0:T(8,128)(2,1)S(1)} %collective-permute-done.3.refs_3_), channel_id=1, source_target_pairs={{0,8},{8,16},{16,24},{24,28},{28,20},{20,12},{12,4},{4,0},{1,9},{9... | collective-permute-start | bytes 393224 | tf_op jit(solution)/shard_map/ppermute | solution.py:275
  48.3 29.4 %collective-permute-start.24 = (bf16[512,512]{1,0:T(8,128)(2,1)S(1)}, bf16[512,512]{1,0:T(8,128)(2,1)S(1)}, u32[]{:S(2)}, u32[]{:S(2)}) collective-permute-start(bf16[512,512]{1,0:T(8,128)(2,1)S(1)} %get-tuple-element.17), channel_id=1, source_target_pairs={{0,2},{1,3},{2,0},{3,1},{4,6},{5,7},{6,4},{7,5},{8,10},{9,11},{10,... | collective-permute-start | bytes 1572872 | tf_op jit(solution)/shard_map/ppermute | solution.py:666
  49.8 6.7 %collective-permute-start.32 = (bf16[256,256]{1,0:T(8,128)(2,1)S(1)}, bf16[256,256]{1,0:T(8,128)(2,1)S(1)}, u32[]{:S(2)}, u32[]{:S(2)}) collective-permute-start(bf16[256,256]{1,0:T(8,128)(2,1)S(1)} %collective-permute-done.31.refs_6_), channel_id=1, source_target_pairs={{8,0},{16,8},{24,16},{28,24},{20,28},{12,20},{4,12},{0,4},{9,1},{1... | collective-permute-start | bytes 393224 | tf_op jit(solution)/shard_map/ppermute | solution.py:278
  51.7 26.1 %collective-permute-start.25 = (bf16[512,512]{1,0:T(8,128)(2,1)S(1)}, bf16[512,512]{1,0:T(8,128)(2,1)S(1)}, u32[]{:S(2)}, u32[]{:S(2)}) collective-permute-start(bf16[512,512]{1,0:T(8,128)(2,1)S(1)} %get-tuple-element.18), channel_id=1, source_target_pairs={{0,3},{1,2},{2,1},{3,0},{4,7},{5,6},{6,5},{7,4},{8,11},{9,10},{10,... | collective-permute-start | bytes 1572872 | tf_op jit(solution)/shard_map/ppermute | solution.py:666
  56.6 25.1 %collective-permute-start.37 = (bf16[512,512]{1,0:T(8,128)(2,1)S(1)}, bf16[512,512]{1,0:T(8,128)(2,1)S(1)}, u32[]{:S(2)}, u32[]{:S(2)}) collective-permute-start(bf16[512,512]{1,0:T(8,128)(2,1)S(1)} %get-tuple-element.22), channel_id=1, source_target_pairs={{0,1},{1,0},{2,3},{3,2},{4,5},{5,4},{6,7},{7,6},{8,9},{9,8},{10,11... | collective-permute-start | bytes 1572872 | tf_op jit(solution)/shard_map/ppermute | solution.py:666
  (33 other events, 316.5 us)
where the time goes:
time: 84.4 us; the launch traced here: 84 us
  starting transfers between devices  35.7 us (42%)
  waiting for transfers between devices  33 us (39%)
  Pallas kernels  9.14 us (11%)
  local copies, waits for them, and re-layouts  5.97 us (7%)
    ppermute x14, starting transfers between devices, step(): self.ahead = lax.ppermute(self.ahead, 'sp', self.forward)  20.9 us
    ppermute x14, waiting for transfers between devices, step(): self.behind = lax.ppermute(self.behind, 'sp', self.backward)  14.7 us
    ppermute x14, starting transfers between devices, step(): self.behind = lax.ppermute(self.behind, 'sp', self.backward)  10.3 us
    pallas_call x11, Pallas kernels, call(): pl.pallas_call(kernel, out_shape=outs if single else tuple(outs), in_spec...  9.14 us
    ppermute x1, waiting for transfers between devices, ring_body(): halo = lax.ppermute(inputs[:, span - HALO // 2:, :], 'sp', shift)  8.3 us
    ppermute x14, waiting for transfers between devices, step(): self.ahead = lax.ppermute(self.ahead, 'sp', self.forward)  5.8 us
    unnamed x38, local copies, waits for them, and re-layouts  5.12 us
    ppermute x6, waiting for transfers between devices, tp_spread(): found[member ^ bit] = lax.ppermute(found[member], 'tp', pairs)  4.16 us
  transfers between devices with their start and end apart: 38, of which 14 were waited for; matrix products, arithmetic and copies ran while one was open for 1% of the time, Pallas kernels for 9%

commit v1 on v0

--- a/solution.py
+++ b/solution.py
@@ -236,9 +236,11 @@
 
 BF16 = jnp.bfloat16
 F32 = jnp.float32
-HALO = 16
+HALO = 8
 STATE_ROWS = 32
 KERNEL_VMEM = 10 << 20
+BEGIN_FLOPS = 20_000_000_000
+KERNEL_FLOPS = 4_000_000_000
 
 
 def ring_positions(count):
@@ -283,7 +285,7 @@
     return pl.BlockSpec(memory_space=pltpu.VMEM)
 
 
-def call(kernel, outs, operands, scratch=()):
+def call(kernel, outs, operands, scratch=(), flops=KERNEL_FLOPS):
     single = not isinstance(outs, (list, tuple))
     return pl.pallas_call(
         kernel,
@@ -291,17 +293,60 @@
         in_specs=[vmem()] * len(operands),
         out_specs=vmem() if single else tuple(vmem() for _ in outs),
         scratch_shapes=list(scratch),
+        cost_estimate=pl.CostEstimate(flops=flops, bytes_accessed=0, transcendentals=0),
         compiler_params=pltpu.CompilerParams(vmem_limit_bytes=KERNEL_VMEM),
     )(*operands)
 
 
-def pack_kernel(key_ref, value_ref, rec_ref, out_ref):
-    at = 0
-    for part_ref in (key_ref, value_ref):
-        size = part_ref.shape[0]
-        out_ref[:, at : at + size] = part_ref[...].astype(F32).T.astype(BF16)
-        at += size
-    out_ref[:, at:] = rec_ref[...]
+def block_diagonal(weight_ref):
+    blocks, size, _ = weight_ref.shape
+    tall = weight_ref[...].reshape(blocks * size, size)
+    tiled = jnp.concatenate([tall] * blocks, axis=1)
+    row = lax.broadcasted_iota(jnp.int32, tiled.shape, 0) // size
+    column = lax.broadcasted_iota(jnp.int32, tiled.shape, 1) // size
+    return jnp.where(row == column, tiled, jnp.zeros_like(tiled))
+
+
+def begin_kernel(out_ref):
+    out_ref[...] = jnp.zeros_like(out_ref)
+
+
+def pack_kernel(_, key_ref, value_ref, rec_ref, out_ref):
+    size = key_ref.shape[0]
+    pair = jnp.concatenate([key_ref[...], value_ref[...]], axis=0)
+    out_ref[:, : 2 * size] = pair.astype(F32).T.astype(BF16)
+    out_ref[:, 2 * size :] = rec_ref[...]
+
+
+TAP_ROW, RATE_ROW, REC_GAIN_ROW, ATT_GAIN_ROW, KEY_GAIN_ROW, QUERY_GAIN_ROW = 0, 8, 9, 10, 11, 12
+
+
+def norm_kernel(rows_ref, gain_ref, decay_ref, input_ref, *refs):
+    taps_ref, *line_refs = refs[:6]
+    normed_ref, tail_ref, gates_ref, small_ref = refs[6:]
+    small_ref[...] = jnp.zeros_like(small_ref)
+    small_ref[TAP_ROW : TAP_ROW + CONV_TAPS, :] = taps_ref[...].astype(F32)
+    for at, line_ref in enumerate(line_refs, RATE_ROW):
+        copies = small_ref.shape[1] // line_ref.shape[1]
+        small_ref[at : at + 1, :] = jnp.concatenate([line_ref[...]] * copies, axis=1)
+    slices, _, width = normed_ref.shape
+    seq_count, span, _ = rows_ref.shape
+    gain = gain_ref[...]
+    tails = []
+    for seq in range(seq_count):
+        values = rms_scale(rows_ref[seq].astype(F32), gain)
+        tails.append(values[span - HALO :])
+        normed = values.astype(BF16)
+        for part in range(slices):
+            normed_ref[part, seq * span : (seq + 1) * span, :] = normed[
+                :, part * width : (part + 1) * width
+            ]
+    tail = jnp.concatenate(tails, axis=0).astype(BF16)
+    for part in range(slices):
+        tail_ref[part] = tail[:, part * width : (part + 1) * width]
+    channels = gates_ref.shape[0]
+    gates_ref[:, :channels] = block_diagonal(decay_ref)
+    gates_ref[:, channels:] = block_diagonal(input_ref)
 
 
 def pack_out_kernel(att_ref, rec_ref, *out_refs):
@@ -314,34 +359,6 @@
         out_ref[rows:, :] = rec_ref[:, columns]
 
 
-def block_diagonal(weight_ref):
-    blocks, size, _ = weight_ref.shape
-    tall = weight_ref[...].reshape(blocks * size, size)
-    tiled = jnp.concatenate([tall] * blocks, axis=1)
-    row = lax.broadcasted_iota(jnp.int32, tiled.shape, 0) // size
-    column = lax.broadcasted_iota(jnp.int32, tiled.shape, 1) // size
-    return jnp.where(row == column, tiled, jnp.zeros_like(tiled))
-
-
-def norm_kernel(rows_ref, halo_ref, gain_ref, decay_ref, input_ref, out_ref, gates_ref):
-    slices, _, width = out_ref.shape
-    seq_count, span, _ = rows_ref.shape
-    gain = gain_ref[...]
-    kept = jnp.where(lax.axis_index("sp") > 0, 1.0, 0.0)
-    for seq in range(seq_count):
-        first = seq * (HALO + span)
-        tail = halo_ref[seq].astype(F32) * kept
-        tail = jnp.concatenate([jnp.zeros_like(tail), tail], axis=0)
-        body_rows = rows_ref[seq].astype(F32)
-        for values, at, size in ((tail, first, HALO), (body_rows, first + HALO, span)):
-            normed = rms_scale(values, gain).astype(BF16)
-            for part in range(slices):
-                out_ref[part, at : at + size, :] = normed[:, part * width : (part + 1) * width]
-    channels = gates_ref.shape[0]
-    gates_ref[:, :channels] = block_diagonal(decay_ref)
-    gates_ref[:, channels:] = block_diagonal(input_ref)
-
-
 def softplus(value):
     small = jnp.exp(-jnp.abs(value))
     series = jnp.full_like(small, 1.0 / 7)
@@ -352,16 +369,20 @@
     )
 
 
-def gathered_dot(normed_ref, weight_refs, count, first=0, total=None):
+def gathered_dot(normed_ref, weight_refs, count, first=0, total=None, halo_ref=None):
     found = arrivals(lax.axis_index("sp"), count)[first:]
     for index, weight_ref in zip(found, weight_refs):
-        term = jnp.dot(normed_ref[index], weight_ref[...], preferred_element_type=F32)
+        rows = normed_ref[index]
+        if halo_ref is not None:
+            rows = jnp.concatenate([rows, halo_ref[index]], axis=0)
+        term = jnp.dot(rows, weight_ref[...], preferred_element_type=F32)
         total = term if total is None else total + term
     return total
 
 
-def part_kernel(count, normed_ref, *refs):
-    refs[-1][...] = gathered_dot(normed_ref, refs[:-1], count)
+def part_kernel(count, with_halo, normed_ref, *refs):
+    halo_ref = refs[0] if with_halo else None
+    refs[-1][...] = gathered_dot(normed_ref, refs[with_halo:-1], count, halo_ref=halo_ref)
 
 
 def minus_expm1(value, exp_value):
@@ -380,12 +401,11 @@
 def recurrence_kernel(count, head_dim, *refs):
     (
         normed_ref,
+        halo_ref,
         part_ref,
         last_ref,
-        key_gain_ref,
-        taps_ref,
+        small_ref,
         gates_ref,
-        decay_param_ref,
         extra_ref,
         message_ref,
         state_ref,
@@ -395,18 +415,22 @@
     ) = refs
     seq_count, span, channels = extra_ref.shape
     kv_width = 2 * head_dim
-    sums = gathered_dot(normed_ref, [last_ref], count, count - 1, part_ref[...])
-    rec_ref[...] = sums[:, kv_width:].astype(BF16).astype(F32)
-    rate = softplus(-decay_param_ref[...])
-    taps = taps_ref[...].astype(F32)
-    key_gain = jnp.concatenate([key_gain_ref[...]] * 2, axis=1)
+    sums = gathered_dot(normed_ref, [last_ref], count, count - 1, part_ref[...], halo_ref)
+    rec_in = sums[:, kv_width:].astype(BF16).astype(F32)
+    kept = jnp.where(lax.axis_index("sp") > 0, 1.0, 0.0)
+    rate = softplus(-small_ref[RATE_ROW : RATE_ROW + 1, :])
+    taps = small_ref[TAP_ROW : TAP_ROW + CONV_TAPS, :]
+    key_gain = small_ref[KEY_GAIN_ROW : KEY_GAIN_ROW + 1, :kv_width]
     lane = lax.broadcasted_iota(jnp.int32, (span, kv_width), 1)
     ends_ref[...] = jnp.zeros_like(ends_ref)
     halves = channels // kv_width
     for seq in range(seq_count):
         first = seq * (HALO + span)
         rows = pl.ds(seq * span, span)
-        kv = sums[first + HALO : first + HALO + span, :kv_width]
+        before = seq_count * span + seq * HALO
+        rec_ref[first : first + HALO, :] = rec_in[before : before + HALO] * kept
+        rec_ref[first + HALO : first + HALO + span, :] = rec_in[seq * span : (seq + 1) * span]
+        kv = sums[seq * span : (seq + 1) * span, :kv_width]
         key = jnp.where(lane < head_dim, kv, 0.0)
         mean = jnp.sum(key * key, axis=-1, keepdims=True) * (1.0 / head_dim)
         scaled = kv * lax.rsqrt(mean + norm_eps) * key_gain
@@ -449,17 +473,16 @@
 
 
 def query_kernel(count, head_dim, seq_count, normed_ref, *refs):
-    query_gain_ref, query_ref = refs[-2:]
+    small_ref, query_ref = refs[-2:]
     width = query_ref.shape[2]
     span = query_ref.shape[1]
     heads = query_ref.shape[0] // seq_count
-    gain = jnp.concatenate([query_gain_ref[...]] * 2, axis=1)
+    gain = small_ref[QUERY_GAIN_ROW : QUERY_GAIN_ROW + 1, :width]
     sums = gathered_dot(normed_ref, refs[:-2], count)
     lane = lax.broadcasted_iota(jnp.int32, (span, width), 1)
     scaling = head_dim ** (-0.5)
     for seq in range(seq_count):
-        first = seq * (HALO + span) + HALO
-        rows = sums[first : first + span]
+        rows = sums[seq * span : (seq + 1) * span]
         for head in range(heads):
             pair = rows[:, head // 2 * width : (head // 2 + 1) * width]
             if head % 2:
@@ -479,7 +502,7 @@
         normed_ref,
         part_ref,
         last_ref,
-        gain_ref,
+        small_ref,
         out_ref,
         ends_ref,
     ) = refs[count:]
@@ -504,7 +527,7 @@
             lanes = slice(half * width, (half + 1) * width)
             at = seq * halves + half
             part = pl.ds(seq * span, span)
-            first = seq * (HALO + span) + HALO
+            first = seq * span
             state = state_ref[part, lanes] + decay_ref[part, lanes] * entering[at : at + 1, :]
             gated = state * jax.nn.gelu(gate[first : first + span, lanes])
             square = gated * gated
@@ -512,26 +535,47 @@
             low = jnp.sum(jnp.where(lane < group, square, 0.0), axis=-1, keepdims=True)
             mean = jnp.where(lane < group, low, total - low) * (1.0 / group)
             out_ref[part, lanes] = (
-                gated * lax.rsqrt(mean + norm_eps) * gain_ref[:, lanes]
+                gated * lax.rsqrt(mean + norm_eps) * small_ref[REC_GAIN_ROW : REC_GAIN_ROW + 1, lanes]
             ).astype(BF16)
 
 
-def attention_kernel(count, head_dim, *refs):
+def lane_sums(value, first=0):
+    lanes = value.shape[1]
+    row = lax.broadcasted_iota(jnp.int32, (lanes, lanes), 0)
+    chosen = jnp.where(row >= first, 1.0, 0.0).astype(BF16)
+    high = value.astype(BF16)
+    low = (value - high.astype(F32)).astype(BF16)
+    return jnp.dot(high, chosen, preferred_element_type=F32) + jnp.dot(
+        low, chosen, preferred_element_type=F32
+    )
+
+
+def attention_kernel(count, head_dim, first, last, *refs):
     query_ref = refs[0]
-    message_refs = refs[1 : 1 + count]
-    gate_ref, gain_ref, out_ref, score_ref = refs[1 + count :]
+    message_refs = refs[1 : 1 + last - first]
+    refs = refs[1 + last - first :]
+    gate_ref = refs[0]
+    before_refs = refs[1:4] if first else None
+    score_ref = refs[-1]
+    if last == count:
+        small_ref, out_ref = refs[-3:-1]
+    else:
+        after_refs = refs[-4:-1]
     span, width = query_ref.shape[1:]
-    rows = out_ref.shape[0]
-    seq_count = rows // span
+    seq_count = gate_ref.shape[0]
     heads = query_ref.shape[0] // seq_count
     place = lax.axis_index("sp")
-    found = arrivals(place, count)
+    found = arrivals(place, count)[first:last]
     ahead = lax.broadcasted_iota(jnp.int32, (span, span), 1) - lax.broadcasted_iota(
         jnp.int32, (span, span), 0
     )
     lane = lax.broadcasted_iota(jnp.int32, (span, width), 1)
     for seq in range(seq_count):
         keys = pl.ds(seq * span, span)
+        lines = [
+            slice((seq * heads + head) * span, (seq * heads + head + 1) * span)
+            for head in range(heads)
+        ]
         queries = query_ref[seq * heads : (seq + 1) * heads].reshape(heads * span, width)
         top = [None] * heads
         own = gate_ref[seq, :, pl.ds(pl.multiple_of(place * span, span), span)]
@@ -552,9 +596,12 @@
                 score_ref[at, head * span : (head + 1) * span, :] = score
                 top[head] = score if at == 0 else jnp.maximum(top[head], score)
         top = [jnp.max(part, axis=-1, keepdims=True) for part in top]
+        if first:
+            top_before = [before_refs[0][line, :] for line in lines]
+            top = [jnp.maximum(part, old) for part, old in zip(top, top_before)]
         totals = [None] * heads
         weighted = None
-        for at in range(count):
+        for at in range(len(found)):
             weights = []
             for head in range(heads):
                 part = jnp.exp(score_ref[at, head * span : (head + 1) * span, :] - top[head])
@@ -568,17 +615,28 @@
             weighted = term if at == 0 else weighted + term
         outs = []
         for head in range(heads):
-            total = jnp.sum(totals[head], axis=-1, keepdims=True)
-            attended = weighted[head * span : (head + 1) * span] / total
-            attended = jnp.where(lane >= head_dim, attended, 0.0)
-            mean = jnp.sum(attended * attended, axis=-1, keepdims=True) * (1.0 / head_dim)
+            total = lane_sums(totals[head])
+            value = weighted[head * span : (head + 1) * span]
+            line = lines[head]
+            if first:
+                fading = jnp.exp(top_before[head] - top[head])
+                total = total + before_refs[1][line, :] * fading
+                value = value + before_refs[2][line, :] * fading
+            if last < count:
+                after_refs[0][line, :] = jnp.broadcast_to(top[head], value.shape)
+                after_refs[1][line, :] = total
+                after_refs[2][line, :] = value
+                continue
+            attended = value * (1.0 / total)
+            mean = lane_sums(attended * attended, head_dim) * (1.0 / head_dim)
             outs.append(attended * lax.rsqrt(mean + norm_eps))
-        for pair in range(heads // 2):
+        for pair in range(len(outs) // 2):
             lanes = slice(pair * width, (pair + 1) * width)
             joined = jnp.where(
                 lane < head_dim, pltpu.roll(outs[2 * pair], head_dim, 1), outs[2 * pair + 1]
             )
-            out_ref[keys, lanes] = (joined * gain_ref[:, lanes]).astype(BF16)
+            gain = small_ref[ATT_GAIN_ROW : ATT_GAIN_ROW + 1, lanes]
+            out_ref[keys, lanes] = (joined * gain).astype(BF16)
 
 
 def output_kernel(uses, has_base, *refs):
@@ -639,35 +697,48 @@
     out_cols = model_width // tp_count
     query_ring = Ring(query_weight, count, False)
     query_ring.step(1)
+    begun = call(begin_kernel, jax.ShapeDtypeStruct((8, 128), F32), [], flops=BEGIN_FLOPS)
     first_chunk = call(
         pack_kernel,
         jax.ShapeDtypeStruct((rec_in_weight.shape[0], width + channels), BF16),
-        [key_weight.T, value_weight.T, rec_in_weight],
+        [begun, key_weight.T, value_weight.T, rec_in_weight],
     )
     first_ring = Ring(first_chunk, count, True)
     first_ring.step(1)
-    shift = [(member, (member + 1) % count) for member in range(count)]
-    halo = lax.ppermute(inputs[:, span - HALO // 2 :, :], "sp", shift)
-
-    normed, gate_weights = call(
+    slice_width = model_width // count
+    normed, tail, gate_weights, small = call(
         norm_kernel,
         [
-            jax.ShapeDtypeStruct((count, ext_rows, model_width // count), BF16),
+            jax.ShapeDtypeStruct((count, rows, slice_width), BF16),
+            jax.ShapeDtypeStruct((count, seq_count * HALO, slice_width), BF16),
             jax.ShapeDtypeStruct((channels, 2 * channels), BF16),
+            jax.ShapeDtypeStruct((16, channels), F32),
         ],
-        [inputs, halo, norm_gain.reshape(1, model_width), decay_gate_weight, input_gate_weight],
-    )
-    out_weight = call(
-        pack_out_kernel,
-        [jax.ShapeDtypeStruct((att_width + channels, out_cols), BF16) for _ in range(tp_count)],
-        [out_att_weight, out_rec_weight],
-    )
-    out_weight = [out_weight[0]] + [
-        lax.ppermute(
-            out_weight[member], "tp", [(source, source ^ member) for source in range(tp_count)]
+        [
+            inputs,
+            norm_gain.reshape(1, model_width),
+            decay_gate_weight,
+            input_gate_weight,
+            conv_weight,
+            decay_param.reshape(1, channels),
+            rec_out_gain.reshape(1, channels),
+            attn_out_gain.reshape(1, att_width),
+            key_gain.reshape(1, head_dim),
+            query_gain.reshape(1, head_dim),
+        ],
+    )
+    out_weight = list(
+        call(
+            pack_out_kernel,
+            [jax.ShapeDtypeStruct((att_width + channels, out_cols), BF16)] * tp_count,
+            [out_att_weight, out_rec_weight],
         )
-        for member in range(1, tp_count)
-    ]
+    )
+    shift = [(member, (member + 1) % count) for member in range(count)]
+    halo = lax.ppermute(tail, "sp", shift)
+    for member in range(1, tp_count):
+        pairs = [(source, source ^ member) for source in range(tp_count)]
+        out_weight[member] = lax.ppermute(out_weight[member], "tp", pairs)
 
     for number in range(2, count // 2 + 1):
         first_ring.step(number)
@@ -676,12 +747,12 @@
     for number in range(1, count // 2 + 1):
         gate_ring.step(number)
 
-    def part_of(ring):
+    def part_of(ring, halos=()):
         columns = ring.blocks[0].shape[1]
         return call(
-            functools.partial(part_kernel, count),
-            jax.ShapeDtypeStruct((ext_rows, columns), F32),
-            [normed, *ring.blocks[:-1]],
+            functools.partial(part_kernel, count, len(halos)),
+            jax.ShapeDtypeStruct((rows + len(halos) * seq_count * HALO, columns), F32),
+            [normed, *halos, *ring.blocks[:-1]],
         )
 
     message, local_state, cum_decay = call(
@@ -693,12 +764,11 @@
         ],
         [
             normed,
-            part_of(first_ring),
+            halo,
+            part_of(first_ring, (halo,)),
             first_ring.blocks[-1],
-            key_gain.reshape(1, head_dim),
-            conv_weight,
+            small,
             gate_weights,
-            decay_param.reshape(1, channels),
             decay_extra,
         ],
         scratch=[pltpu.VMEM((ext_rows, channels), F32), pltpu.VMEM((8, width), F32)],
@@ -710,7 +780,7 @@
     queries = call(
         functools.partial(query_kernel, count, head_dim, seq_count),
         jax.ShapeDtypeStruct((seq_count * heads, span, width), BF16),
-        [normed, *query_ring.blocks, query_gain.reshape(1, head_dim)],
+        [normed, *query_ring.blocks, small],
     )
     messages = message_ring.blocks
     rec_normed = call(
@@ -723,15 +793,22 @@
             normed,
             part_of(gate_ring),
             gate_ring.blocks[-1],
-            rec_out_gain.reshape(1, channels),
+            small,
         ],
         scratch=[pltpu.VMEM((count, 8, width), F32)],
     )
+    early = count - 1
+    attended = call(
+        functools.partial(attention_kernel, count, head_dim, 0, early),
+        [jax.ShapeDtypeStruct((seq_count * heads * span, width), F32)] * 3,
+        [queries, *messages[:early], forget_cache],
+        scratch=[pltpu.VMEM((early, heads * span, span), F32)],
+    )
     att_normed = call(
-        functools.partial(attention_kernel, count, head_dim),
+        functools.partial(attention_kernel, count, head_dim, early, count),
         jax.ShapeDtypeStruct((rows, att_width), BF16),
-        [queries, *messages, forget_cache, attn_out_gain.reshape(1, att_width)],
-        scratch=[pltpu.VMEM((count, heads * span, span), F32)],
+        [queries, *messages[early:], forget_cache, *attended, small],
+        scratch=[pltpu.VMEM((count - early, heads * span, span), F32)],
     )
 
     def project(rec_members, att_members, base, kind):

time: 84.4 us -> 77.4 us (0.917)
  waiting for transfers between devices: 33 us -> 27.5 us
  local copies, waits for them, and re-layouts: 5.97 us -> 1.63 us
  starting transfers between devices: 35.7 us -> 37.8 us
  Pallas kernels: 9.14 us -> 10.1 us
    ppermute x4, waiting for transfers between devices: 8.31 us -> 4.22 us  [the longest x1 4.21 us: ring_body(): halo = lax.ppermute(tail, 'sp', shift)]
    ppermute x14, waiting for transfers between devices: 14.7 us -> 10.7 us  [step(): self.behind = lax.ppermute(self.behind, 'sp', self.backward)]
    unnamed x38, local copies, waits for them, and re-layouts: 5.12 us -> 1.63 us
    ppermute x14, waiting for transfers between devices: 5.8 us -> 8.96 us  [step(): self.ahead = lax.ppermute(self.ahead, 'sp', self.forward)]
    ppermute x14, starting transfers between devices: 10.3 us -> 7.4 us  [step(): self.behind = lax.ppermute(self.behind, 'sp', self.backward)]
    ppermute x4, starting transfers between devices: 1.82 us -> 4.49 us  [the longest x3 2.48 us: ring_body(): out_weight[member] = lax.ppermute(out_weight[member], 'tp', pairs)]
    ppermute x14, starting transfers between devices: 20.9 us -> 23.2 us  [step(): self.ahead = lax.ppermute(self.ahead, 'sp', self.forward)]
    pallas_call x11 -> x13, Pallas kernels: 9.14 us -> 10.1 us  [call(): pl.pallas_call(kernel, out_shape=outs if single else tuple(outs), in_spec...]
  transfers between devices with their start and end apart: 38 -> 38, of which waited for: 14 -> 15; matrix products, arithmetic and copies ran while one was open for 1% -> 0% of each run, Pallas kernels for 9% -> 12%
where the time goes in v1:
time: 77.4 us; the launch traced here: 77.2 us
  starting transfers between devices  37.8 us (49%)
  waiting for transfers between devices  27.5 us (36%)
  Pallas kernels  10.1 us (13%)
  local copies, waits for them, and re-layouts  1.63 us (2%)
    ppermute x14, starting transfers between devices, step(): self.ahead = lax.ppermute(self.ahead, 'sp', self.forward)  23.2 us
    ppermute x14, waiting for transfers between devices, step(): self.behind = lax.ppermute(self.behind, 'sp', self.backward)  10.7 us
    pallas_call x13, Pallas kernels, call(): pl.pallas_call(kernel, out_shape=outs if single else tuple(outs), in_spec...  10.1 us
    ppermute x14, waiting for transfers between devices, step(): self.ahead = lax.ppermute(self.ahead, 'sp', self.forward)  8.96 us
    ppermute x14, starting transfers between devices, step(): self.behind = lax.ppermute(self.behind, 'sp', self.backward)  7.4 us
    ppermute x1, waiting for transfers between devices, ring_body(): halo = lax.ppermute(tail, 'sp', shift)  4.21 us
    ppermute x6, waiting for transfers between devices, tp_spread(): found[member ^ bit] = lax.ppermute(found[member], 'tp', pairs)  3.61 us
    ppermute x6, starting transfers between devices, tp_spread(): found[member ^ bit] = lax.ppermute(found[member], 'tp', pairs)  2.67 us
  transfers between devices with their start and end apart: 38, of which 15 were waited for; matrix products, arithmetic and copies ran while one was open for 0% of the time, Pallas kernels for 12%

profile of v1, /device:TPU:0, one launch (start us, length us, event | category | flops | bytes accessed | tf_op | source)
XLA Modules:
  0.0 77.2 jit_solution(13525322957288100899)
XLA Ops:
  1.1 3.1 %collective-permute-start.8 = (bf16[256,384]{1,0:T(8,128)(2,1)S(1)}, bf16[256,384]{1,0:T(8,128)(2,1)S(1)}, u32[]{:S(2)}, u32[]{:S(2)}) collective-permute-start(bf16[256,384]{1,0:T(8,128)(2,1)S(1)} %shard_map.184.refs_1_), channel_id=1, source_target_pairs={{0,8},{8,16},{16,24},{24,28},{28,20},{20,12},{12,4},{4,0},{1,9},{9... | collective-permute-start | bytes 589832 | tf_op jit(solution)/shard_map/ppermute | solution.py:277
  4.2 2.0 %collective-permute-start.27 = (bf16[256,256]{1,0:T(8,128)(2,1)S(1)}, bf16[256,256]{1,0:T(8,128)(2,1)S(1)}, u32[]{:S(2)}, u32[]{:S(2)}) collective-permute-start(bf16[256,256]{1,0:T(8,128)(2,1)S(1)} %copy-done.5), channel_id=1, source_target_pairs={{8,0},{16,8},{24,16},{28,24},{20,28},{12,20},{4,12},{0,4},{9,1},{1... | collective-permute-start | bytes 393224 | tf_op jit(solution)/shard_map/ppermute | solution.py:280
  6.2 2.9 %collective-permute-done.8.refs_2_ = bf16[256,384]{1,0:T(8,128)(2,1)S(1)} collective-permute-done((bf16[256,384]{1,0:T(8,128)(2,1)S(1)}, bf16[256,384]{1,0:T(8,128)(2,1)S(1)}, u32[]{:S(2)}, u32[]{:S(2)}) %collective-permute-start.8) | collective-permute-done | bytes 196640 | tf_op jit(solution)/shard_map/ppermute | solution.py:277
  9.1 1.8 %collective-permute-start.10 = (bf16[256,384]{1,0:T(8,128)(2,1)S(1)}, bf16[256,384]{1,0:T(8,128)(2,1)S(1)}, u32[]{:S(2)}, u32[]{:S(2)}) collective-permute-start(bf16[256,384]{1,0:T(8,128)(2,1)S(1)} %collective-permute-done.8.refs_2_), channel_id=1, source_target_pairs={{0,8},{8,16},{16,24},{24,28},{28,20},{20,12},{12,4},{4,0},{1,9},{9... | collective-permute-start | bytes 589832 | tf_op jit(solution)/shard_map/ppermute | solution.py:277
  13.2 2.0 %collective-permute-start.7 = (bf16[8,16,256]{2,1,0:T(8,128)(2,1)S(1)}, bf16[8,16,256]{2,1,0:T(8,128)(2,1)S(1)}, u32[]{:S(2)}, u32[]{:S(2)}) collective-permute-start(bf16[8,16,256]{2,1,0:T(8,128)(2,1)S(1)} %get-tuple-element.21), channel_id=1, source_target_pairs={{0,4},{4,8},{8,12},{12,16},{16,20},{20,24},{24,28},{28,0},{1,5},{5... | collective-permute-start | bytes 196616 | tf_op jit(solution)/shard_map/ppermute | solution.py:738
  15.2 1.6 %collective-permute-start.26 = (bf16[256,256]{1,0:T(8,128)(2,1)S(1)}, bf16[256,256]{1,0:T(8,128)(2,1)S(1)}, u32[]{:S(2)}, u32[]{:S(2)}) collective-permute-start(bf16[256,256]{1,0:T(8,128)(2,1)S(1)} %copy-done.5), channel_id=1, source_target_pairs={{0,8},{8,16},{16,24},{24,28},{28,20},{20,12},{12,4},{4,0},{1,9},{9... | collective-permute-start | bytes 393224 | tf_op jit(solution)/shard_map/ppermute | solution.py:277
  16.8 4.2 %collective-permute-done.7.refs_0_.refs_1_ = bf16[8,16,256]{2,1,0:T(8,128)(2,1)S(1)} collective-permute-done((bf16[8,16,256]{2,1,0:T(8,128)(2,1)S(1)}, bf16[8,16,256]{2,1,0:T(8,128)(2,1)S(1)}, u32[]{:S(2)}, u32[]{:S(2)}) %collective-permute-start.7) | collective-permute-done | bytes 65568 | tf_op jit(solution)/shard_map/ppermute | solution.py:738
  21.0 2.0 %collective-permute-start = (bf16[256,256]{1,0:T(8,128)(2,1)S(1)}, bf16[256,256]{1,0:T(8,128)(2,1)S(1)}, u32[]{:S(2)}, u32[]{:S(2)}) collective-permute-start(bf16[256,256]{1,0:T(8,128)(2,1)S(1)} %copy-done.6), channel_id=1, source_target_pairs={{0,8},{8,16},{16,24},{24,28},{28,20},{20,12},{12,4},{4,0},{1,9},{9... | collective-permute-start | bytes 393224 | tf_op jit(solution)/shard_map/ppermute | solution.py:277
  23.1 2.0 %collective-permute-start.13 = (bf16[256,384]{1,0:T(8,128)(2,1)S(1)}, bf16[256,384]{1,0:T(8,128)(2,1)S(1)}, u32[]{:S(2)}, u32[]{:S(2)}) collective-permute-start(bf16[256,384]{1,0:T(8,128)(2,1)S(1)} %collective-permute-done.11.refs_5_), channel_id=1, source_target_pairs={{8,0},{16,8},{24,16},{28,24},{20,28},{12,20},{4,12},{0,4},{9,1},{1... | collective-permute-start | bytes 589832 | tf_op jit(solution)/shard_map/ppermute | solution.py:280
  25.1 2.2 %collective-permute-done.1.refs_2_ = bf16[256,256]{1,0:T(8,128)(2,1)S(1)} collective-permute-done((bf16[256,256]{1,0:T(8,128)(2,1)S(1)}, bf16[256,256]{1,0:T(8,128)(2,1)S(1)}, u32[]{:S(2)}, u32[]{:S(2)}) %collective-permute-start.1) | collective-permute-done | bytes 131104 | tf_op jit(solution)/shard_map/ppermute | solution.py:280
  27.4 2.0 %collective-permute-start.3 = (bf16[256,256]{1,0:T(8,128)(2,1)S(1)}, bf16[256,256]{1,0:T(8,128)(2,1)S(1)}, u32[]{:S(2)}, u32[]{:S(2)}) collective-permute-start(bf16[256,256]{1,0:T(8,128)(2,1)S(1)} %collective-permute-done.1.refs_2_), channel_id=1, source_target_pairs={{8,0},{16,8},{24,16},{28,24},{20,28},{12,20},{4,12},{0,4},{9,1},{1... | collective-permute-start | bytes 393224 | tf_op jit(solution)/shard_map/ppermute | solution.py:280
  29.4 2.8 %collective-permute-done.29.refs_4_ = bf16[256,256]{1,0:T(8,128)(2,1)S(1)} collective-permute-done((bf16[256,256]{1,0:T(8,128)(2,1)S(1)}, bf16[256,256]{1,0:T(8,128)(2,1)S(1)}, u32[]{:S(2)}, u32[]{:S(2)}) %collective-permute-start.29) | collective-permute-done | bytes 131104 | tf_op jit(solution)/shard_map/ppermute | solution.py:280
  37.0 2.1 %collective-permute-start.14 = (bf16[256,384]{1,0:T(8,128)(2,1)S(1)}, bf16[256,384]{1,0:T(8,128)(2,1)S(1)}, u32[]{:S(2)}, u32[]{:S(2)}) collective-permute-start(bf16[256,384]{1,0:T(8,128)(2,1)S(1)} %collective-permute-done.12.refs_6_), channel_id=1, source_target_pairs={{0,8},{8,16},{16,24},{24,28},{28,20},{20,12},{12,4},{4,0},{1,9},{9... | collective-permute-start | bytes 589832 | tf_op jit(solution)/shard_map/ppermute | solution.py:277
  39.8 3.7 %collective-permute-done.14.refs_3_ = bf16[256,384]{1,0:T(8,128)(2,1)S(1)} collective-permute-done((bf16[256,384]{1,0:T(8,128)(2,1)S(1)}, bf16[256,384]{1,0:T(8,128)(2,1)S(1)}, u32[]{:S(2)}, u32[]{:S(2)}) %collective-permute-start.14) | collective-permute-done | bytes 196640 | tf_op jit(solution)/shard_map/ppermute | solution.py:277
  44.8 2.1 %collective-permute-start.15 = (bf16[288,128]{1,0:T(8,128)(2,1)S(1)}, bf16[288,128]{1,0:T(8,128)(2,1)S(1)}, u32[]{:S(2)}, u32[]{:S(2)}) collective-permute-start(bf16[288,128]{1,0:T(8,128)(2,1)S(1)} %get-tuple-element.23.refs_1_.refs_0_), channel_id=1, source_target_pairs={{0,8},{8,16},{16,24},{24,28},{28,20},{20,12},{12,4},{4,0},{1,9},{9... | collective-permute-start | bytes 221192 | tf_op jit(solution)/shard_map/ppermute | solution.py:277
  47.1 2.5 %collective-permute-start.24 = (bf16[512,512]{1,0:T(8,128)(2,1)S(1)}, bf16[512,512]{1,0:T(8,128)(2,1)S(1)}, u32[]{:S(2)}, u32[]{:S(2)}) collective-permute-start(bf16[512,512]{1,0:T(8,128)(2,1)S(1)} %get-tuple-element.27), channel_id=1, source_target_pairs={{0,2},{1,3},{2,0},{3,1},{4,6},{5,7},{6,4},{7,5},{8,10},{9,11},{10,... | collective-permute-start | bytes 1572872 | tf_op jit(solution)/shard_map/ppermute | solution.py:741
  49.5 2.1 %collective-permute-start.4 = (bf16[256,256]{1,0:T(8,128)(2,1)S(1)}, bf16[256,256]{1,0:T(8,128)(2,1)S(1)}, u32[]{:S(2)}, u32[]{:S(2)}) collective-permute-start(bf16[256,256]{1,0:T(8,128)(2,1)S(1)} %collective-permute-done.2.refs_3_), channel_id=1, source_target_pairs={{0,8},{8,16},{16,24},{24,28},{28,20},{20,12},{12,4},{4,0},{1,9},{9... | collective-permute-start | bytes 393224 | tf_op jit(solution)/shard_map/ppermute | solution.py:277
  51.7 2.1 %collective-permute-start.16 = (bf16[288,128]{1,0:T(8,128)(2,1)S(1)}, bf16[288,128]{1,0:T(8,128)(2,1)S(1)}, u32[]{:S(2)}, u32[]{:S(2)}) collective-permute-start(bf16[288,128]{1,0:T(8,128)(2,1)S(1)} %collective-permute-done.15.refs_2_.refs_1_), channel_id=1, source_target_pairs={{0,8},{8,16},{16,24},{24,28},{28,20},{20,12},{12,4},{4,0},{1,9},{9... | collective-permute-start | bytes 221192 | tf_op jit(solution)/shard_map/ppermute | solution.py:277
  54.5 2.1 %collective-permute-done.6.refs_7_ = bf16[256,256]{1,0:T(8,128)(2,1)S(1)} collective-permute-done((bf16[256,256]{1,0:T(8,128)(2,1)S(1)}, bf16[256,256]{1,0:T(8,128)(2,1)S(1)}, u32[]{:S(2)}, u32[]{:S(2)}) %collective-permute-start.6) | collective-permute-done | bytes 131104 | tf_op jit(solution)/shard_map/ppermute | solution.py:280
  56.6 2.1 %collective-permute-start.17 = (bf16[288,128]{1,0:T(8,128)(2,1)S(1)}, bf16[288,128]{1,0:T(8,128)(2,1)S(1)}, u32[]{:S(2)}, u32[]{:S(2)}) collective-permute-start(bf16[288,128]{1,0:T(8,128)(2,1)S(1)} %collective-permute-done.16.refs_4_.refs_3_), channel_id=1, source_target_pairs={{0,8},{8,16},{16,24},{24,28},{28,20},{20,12},{12,4},{4,0},{1,9},{9... | collective-permute-start | bytes 221192 | tf_op jit(solution)/shard_map/ppermute | solution.py:277
  59.8 1.5 %collective-permute-done.17.refs_6_.refs_5_ = bf16[288,128]{1,0:T(8,128)(2,1)S(1)} collective-permute-done((bf16[288,128]{1,0:T(8,128)(2,1)S(1)}, bf16[288,128]{1,0:T(8,128)(2,1)S(1)}, u32[]{:S(2)}, u32[]{:S(2)}) %collective-permute-start.17) | collective-permute-done | bytes 73760 | tf_op jit(solution)/shard_map/ppermute | solution.py:277
  61.5 1.6 %collective-permute-done.21.refs_7_.refs_6_ = bf16[288,128]{1,0:T(8,128)(2,1)S(1)} collective-permute-done((bf16[288,128]{1,0:T(8,128)(2,1)S(1)}, bf16[288,128]{1,0:T(8,128)(2,1)S(1)}, u32[]{:S(2)}, u32[]{:S(2)}) %collective-permute-start.21) | collective-permute-done | bytes 73760 | tf_op jit(solution)/shard_map/ppermute | solution.py:280
  64.4 2.5 %shard_map.187 = (f32[1024,128]{1,0:T(8,128)S(1)}, f32[1024,128]{1,0:T(8,128)S(1)}, f32[1024,128]{1,0:T(8,128)S(1)}) custom-call(bf16[8,128,128]{2,1,0:T(8,128)(2,1)S(1)} %shard_map.182.refs_0_, bf16[288,128]{1,0:T(8,128)(2,1)S(1)} %get-tuple-element.23.refs_1_.refs_0_, bf16[288,128]{1,0:T(8,128)(2,1)S(1)} %collective-permute-done.15.refs_2_.refs_1_, ...), custom_call_target="tpu_custom_call" | custom-call | flops 4000000000 | tf_op jit(solution)/shard_map/pallas_call | solution.py:290
  69.6 1.9 %collective-permute-start.22 = (bf16[256,256]{1,0:T(8,128)(2,1)S(1)}, bf16[256,256]{1,0:T(8,128)(2,1)S(1)}, u32[]{:S(2)}, u32[]{:S(2)}) collective-permute-start(bf16[256,256]{1,0:T(8,128)(2,1)S(1)} %shard_map.188.refs_4_), channel_id=1, source_target_pairs={{0,2},{1,3},{2,0},{3,1},{4,6},{5,7},{6,4},{7,5},{8,10},{9,11},{10,... | collective-permute-start | bytes 393224 | tf_op jit(solution)/shard_map/ppermute | solution.py:662
  (103 shorter events, 22.2 us)
Async XLA Ops:
  1.1 7.9 %collective-permute-start.8 = (bf16[256,384]{1,0:T(8,128)(2,1)S(1)}, bf16[256,384]{1,0:T(8,128)(2,1)S(1)}, u32[]{:S(2)}, u32[]{:S(2)}) collective-permute-start(bf16[256,384]{1,0:T(8,128)(2,1)S(1)} %shard_map.184.refs_1_), channel_id=1, source_target_pairs={{0,8},{8,16},{16,24},{24,28},{28,20},{20,12},{12,4},{4,0},{1,9},{9... | collective-permute-start | bytes 589832 | tf_op jit(solution)/shard_map/ppermute | solution.py:277
  4.2 7.8 %collective-permute-start.9 = (bf16[256,384]{1,0:T(8,128)(2,1)S(1)}, bf16[256,384]{1,0:T(8,128)(2,1)S(1)}, u32[]{:S(2)}, u32[]{:S(2)}) collective-permute-start(bf16[256,384]{1,0:T(8,128)(2,1)S(1)} %shard_map.184.refs_1_), channel_id=1, source_target_pairs={{8,0},{16,8},{24,16},{28,24},{20,28},{12,20},{4,12},{0,4},{9,1},{1... | collective-permute-start | bytes 589832 | tf_op jit(solution)/shard_map/ppermute | solution.py:280
  4.2 16.7 %collective-permute-start.27 = (bf16[256,256]{1,0:T(8,128)(2,1)S(1)}, bf16[256,256]{1,0:T(8,128)(2,1)S(1)}, u32[]{:S(2)}, u32[]{:S(2)}) collective-permute-start(bf16[256,256]{1,0:T(8,128)(2,1)S(1)} %copy-done.5), channel_id=1, source_target_pairs={{8,0},{16,8},{24,16},{28,24},{20,28},{12,20},{4,12},{0,4},{9,1},{1... | collective-permute-start | bytes 393224 | tf_op jit(solution)/shard_map/ppermute | solution.py:280
  9.1 13.9 %collective-permute-start.10 = (bf16[256,384]{1,0:T(8,128)(2,1)S(1)}, bf16[256,384]{1,0:T(8,128)(2,1)S(1)}, u32[]{:S(2)}, u32[]{:S(2)}) collective-permute-start(bf16[256,384]{1,0:T(8,128)(2,1)S(1)} %collective-permute-done.8.refs_2_), channel_id=1, source_target_pairs={{0,8},{8,16},{16,24},{24,28},{28,20},{20,12},{12,4},{4,0},{1,9},{9... | collective-permute-start | bytes 589832 | tf_op jit(solution)/shard_map/ppermute | solution.py:277
  12.0 11.1 %collective-permute-start.11 = (bf16[256,384]{1,0:T(8,128)(2,1)S(1)}, bf16[256,384]{1,0:T(8,128)(2,1)S(1)}, u32[]{:S(2)}, u32[]{:S(2)}) collective-permute-start(bf16[256,384]{1,0:T(8,128)(2,1)S(1)} %collective-permute-done.9.refs_3_), channel_id=1, source_target_pairs={{8,0},{16,8},{24,16},{28,24},{20,28},{12,20},{4,12},{0,4},{9,1},{1... | collective-permute-start | bytes 589832 | tf_op jit(solution)/shard_map/ppermute | solution.py:280
  13.2 7.8 %collective-permute-start.7 = (bf16[8,16,256]{2,1,0:T(8,128)(2,1)S(1)}, bf16[8,16,256]{2,1,0:T(8,128)(2,1)S(1)}, u32[]{:S(2)}, u32[]{:S(2)}) collective-permute-start(bf16[8,16,256]{2,1,0:T(8,128)(2,1)S(1)} %get-tuple-element.21), channel_id=1, source_target_pairs={{0,4},{4,8},{8,12},{12,16},{16,20},{20,24},{24,28},{28,0},{1,5},{5... | collective-permute-start | bytes 196616 | tf_op jit(solution)/shard_map/ppermute | solution.py:738
  15.2 9.9 %collective-permute-start.26 = (bf16[256,256]{1,0:T(8,128)(2,1)S(1)}, bf16[256,256]{1,0:T(8,128)(2,1)S(1)}, u32[]{:S(2)}, u32[]{:S(2)}) collective-permute-start(bf16[256,256]{1,0:T(8,128)(2,1)S(1)} %copy-done.5), channel_id=1, source_target_pairs={{0,8},{8,16},{16,24},{24,28},{28,20},{20,12},{12,4},{4,0},{1,9},{9... | collective-permute-start | bytes 393224 | tf_op jit(solution)/shard_map/ppermute | solution.py:277
  21.0 6.4 %collective-permute-start.1 = (bf16[256,256]{1,0:T(8,128)(2,1)S(1)}, bf16[256,256]{1,0:T(8,128)(2,1)S(1)}, u32[]{:S(2)}, u32[]{:S(2)}) collective-permute-start(bf16[256,256]{1,0:T(8,128)(2,1)S(1)} %copy-done.6), channel_id=1, source_target_pairs={{8,0},{16,8},{24,16},{28,24},{20,28},{12,20},{4,12},{0,4},{9,1},{1... | collective-permute-start | bytes 393224 | tf_op jit(solution)/shard_map/ppermute | solution.py:280
  21.0 6.4 %collective-permute-start = (bf16[256,256]{1,0:T(8,128)(2,1)S(1)}, bf16[256,256]{1,0:T(8,128)(2,1)S(1)}, u32[]{:S(2)}, u32[]{:S(2)}) collective-permute-start(bf16[256,256]{1,0:T(8,128)(2,1)S(1)} %copy-done.6), channel_id=1, source_target_pairs={{0,8},{8,16},{16,24},{24,28},{28,20},{20,12},{12,4},{4,0},{1,9},{9... | collective-permute-start | bytes 393224 | tf_op jit(solution)/shard_map/ppermute | solution.py:277
  23.0 13.5 %collective-permute-start.12 = (bf16[256,384]{1,0:T(8,128)(2,1)S(1)}, bf16[256,384]{1,0:T(8,128)(2,1)S(1)}, u32[]{:S(2)}, u32[]{:S(2)}) collective-permute-start(bf16[256,384]{1,0:T(8,128)(2,1)S(1)} %collective-permute-done.10.refs_4_), channel_id=1, source_target_pairs={{0,8},{8,16},{16,24},{24,28},{28,20},{20,12},{12,4},{4,0},{1,9},{9... | collective-permute-start | bytes 589832 | tf_op jit(solution)/shard_map/ppermute | solution.py:277
  23.1 14.0 %collective-permute-start.13 = (bf16[256,384]{1,0:T(8,128)(2,1)S(1)}, bf16[256,384]{1,0:T(8,128)(2,1)S(1)}, u32[]{:S(2)}, u32[]{:S(2)}) collective-permute-start(bf16[256,384]{1,0:T(8,128)(2,1)S(1)} %collective-permute-done.11.refs_5_), channel_id=1, source_target_pairs={{8,0},{16,8},{24,16},{28,24},{20,28},{12,20},{4,12},{0,4},{9,1},{1... | collective-permute-start | bytes 589832 | tf_op jit(solution)/shard_map/ppermute | solution.py:280
  25.0 7.2 %collective-permute-start.29 = (bf16[256,256]{1,0:T(8,128)(2,1)S(1)}, bf16[256,256]{1,0:T(8,128)(2,1)S(1)}, u32[]{:S(2)}, u32[]{:S(2)}) collective-permute-start(bf16[256,256]{1,0:T(8,128)(2,1)S(1)} %collective-permute-done.27.refs_2_), channel_id=1, source_target_pairs={{8,0},{16,8},{24,16},{28,24},{20,28},{12,20},{4,12},{0,4},{9,1},{1... | collective-permute-start | bytes 393224 | tf_op jit(solution)/shard_map/ppermute | solution.py:280
  27.4 6.3 %collective-permute-start.28 = (bf16[256,256]{1,0:T(8,128)(2,1)S(1)}, bf16[256,256]{1,0:T(8,128)(2,1)S(1)}, u32[]{:S(2)}, u32[]{:S(2)}) collective-permute-start(bf16[256,256]{1,0:T(8,128)(2,1)S(1)} %collective-permute-done.26.refs_1_), channel_id=1, source_target_pairs={{0,8},{8,16},{16,24},{24,28},{28,20},{20,12},{12,4},{4,0},{1,9},{9... | collective-permute-start | bytes 393224 | tf_op jit(solution)/shard_map/ppermute | solution.py:277
  27.4 7.7 %collective-permute-start.3 = (bf16[256,256]{1,0:T(8,128)(2,1)S(1)}, bf16[256,256]{1,0:T(8,128)(2,1)S(1)}, u32[]{:S(2)}, u32[]{:S(2)}) collective-permute-start(bf16[256,256]{1,0:T(8,128)(2,1)S(1)} %collective-permute-done.1.refs_2_), channel_id=1, source_target_pairs={{8,0},{16,8},{24,16},{28,24},{20,28},{12,20},{4,12},{0,4},{9,1},{1... | collective-permute-start | bytes 393224 | tf_op jit(solution)/shard_map/ppermute | solution.py:280
  32.2 14.7 %collective-permute-start.2 = (bf16[256,256]{1,0:T(8,128)(2,1)S(1)}, bf16[256,256]{1,0:T(8,128)(2,1)S(1)}, u32[]{:S(2)}, u32[]{:S(2)}) collective-permute-start(bf16[256,256]{1,0:T(8,128)(2,1)S(1)} %collective-permute-done.refs_1_), channel_id=1, source_target_pairs={{0,8},{8,16},{16,24},{24,28},{28,20},{20,12},{12,4},{4,0},{1,9},{9... | collective-permute-start | bytes 393224 | tf_op jit(solution)/shard_map/ppermute | solution.py:277
  33.6 13.4 %collective-permute-start.31 = (bf16[256,256]{1,0:T(8,128)(2,1)S(1)}, bf16[256,256]{1,0:T(8,128)(2,1)S(1)}, u32[]{:S(2)}, u32[]{:S(2)}) collective-permute-start(bf16[256,256]{1,0:T(8,128)(2,1)S(1)} %collective-permute-done.29.refs_4_), channel_id=1, source_target_pairs={{8,0},{16,8},{24,16},{28,24},{20,28},{12,20},{4,12},{0,4},{9,1},{1... | collective-permute-start | bytes 393224 | tf_op jit(solution)/shard_map/ppermute | solution.py:280
  35.0 14.5 %collective-permute-start.30 = (bf16[256,256]{1,0:T(8,128)(2,1)S(1)}, bf16[256,256]{1,0:T(8,128)(2,1)S(1)}, u32[]{:S(2)}, u32[]{:S(2)}) collective-permute-start(bf16[256,256]{1,0:T(8,128)(2,1)S(1)} %collective-permute-done.28.refs_3_), channel_id=1, source_target_pairs={{0,8},{8,16},{16,24},{24,28},{28,20},{20,12},{12,4},{4,0},{1,9},{9... | collective-permute-start | bytes 393224 | tf_op jit(solution)/shard_map/ppermute | solution.py:277
  36.5 15.2 %collective-permute-start.5 = (bf16[256,256]{1,0:T(8,128)(2,1)S(1)}, bf16[256,256]{1,0:T(8,128)(2,1)S(1)}, u32[]{:S(2)}, u32[]{:S(2)}) collective-permute-start(bf16[256,256]{1,0:T(8,128)(2,1)S(1)} %collective-permute-done.3.refs_4_), channel_id=1, source_target_pairs={{8,0},{16,8},{24,16},{28,24},{20,28},{12,20},{4,12},{0,4},{9,1},{1... | collective-permute-start | bytes 393224 | tf_op jit(solution)/shard_map/ppermute | solution.py:280
  37.0 6.5 %collective-permute-start.14 = (bf16[256,384]{1,0:T(8,128)(2,1)S(1)}, bf16[256,384]{1,0:T(8,128)(2,1)S(1)}, u32[]{:S(2)}, u32[]{:S(2)}) collective-permute-start(bf16[256,384]{1,0:T(8,128)(2,1)S(1)} %collective-permute-done.12.refs_6_), channel_id=1, source_target_pairs={{0,8},{8,16},{16,24},{24,28},{28,20},{20,12},{12,4},{4,0},{1,9},{9... | collective-permute-start | bytes 589832 | tf_op jit(solution)/shard_map/ppermute | solution.py:277
  44.8 6.9 %collective-permute-start.15 = (bf16[288,128]{1,0:T(8,128)(2,1)S(1)}, bf16[288,128]{1,0:T(8,128)(2,1)S(1)}, u32[]{:S(2)}, u32[]{:S(2)}) collective-permute-start(bf16[288,128]{1,0:T(8,128)(2,1)S(1)} %get-tuple-element.23.refs_1_.refs_0_), channel_id=1, source_target_pairs={{0,8},{8,16},{16,24},{24,28},{28,20},{20,12},{12,4},{4,0},{1,9},{9... | collective-permute-start | bytes 221192 | tf_op jit(solution)/shard_map/ppermute | solution.py:277
  46.9 6.9 %collective-permute-start.19 = (bf16[288,128]{1,0:T(8,128)(2,1)S(1)}, bf16[288,128]{1,0:T(8,128)(2,1)S(1)}, u32[]{:S(2)}, u32[]{:S(2)}) collective-permute-start(bf16[288,128]{1,0:T(8,128)(2,1)S(1)} %get-tuple-element.23.refs_1_.refs_0_), channel_id=1, source_target_pairs={{8,0},{16,8},{24,16},{28,24},{20,28},{12,20},{4,12},{0,4},{9,1},{1... | collective-permute-start | bytes 221192 | tf_op jit(solution)/shard_map/ppermute | solution.py:280
  47.1 24.4 %collective-permute-start.24 = (bf16[512,512]{1,0:T(8,128)(2,1)S(1)}, bf16[512,512]{1,0:T(8,128)(2,1)S(1)}, u32[]{:S(2)}, u32[]{:S(2)}) collective-permute-start(bf16[512,512]{1,0:T(8,128)(2,1)S(1)} %get-tuple-element.27), channel_id=1, source_target_pairs={{0,2},{1,3},{2,0},{3,1},{4,6},{5,7},{6,4},{7,5},{8,10},{9,11},{10,... | collective-permute-start | bytes 1572872 | tf_op jit(solution)/shard_map/ppermute | solution.py:741
  54.5 17.0 %collective-permute-start.25 = (bf16[512,512]{1,0:T(8,128)(2,1)S(1)}, bf16[512,512]{1,0:T(8,128)(2,1)S(1)}, u32[]{:S(2)}, u32[]{:S(2)}) collective-permute-start(bf16[512,512]{1,0:T(8,128)(2,1)S(1)} %get-tuple-element.28), channel_id=1, source_target_pairs={{0,3},{1,2},{2,1},{3,0},{4,7},{5,6},{6,5},{7,4},{8,11},{9,10},{10,... | collective-permute-start | bytes 1572872 | tf_op jit(solution)/shard_map/ppermute | solution.py:741
  56.6 18.2 %collective-permute-start.37 = (bf16[512,512]{1,0:T(8,128)(2,1)S(1)}, bf16[512,512]{1,0:T(8,128)(2,1)S(1)}, u32[]{:S(2)}, u32[]{:S(2)}) collective-permute-start(bf16[512,512]{1,0:T(8,128)(2,1)S(1)} %get-tuple-element.32), channel_id=1, source_target_pairs={{0,1},{1,0},{2,3},{3,2},{4,5},{5,4},{6,7},{7,6},{8,9},{9,8},{10,11... | collective-permute-start | bytes 1572872 | tf_op jit(solution)/shard_map/ppermute | solution.py:741
  (33 other events, 182.0 us)

commit v2 on v1

--- a/solution.py
+++ b/solution.py
@@ -335,7 +335,7 @@
     tails = []
     for seq in range(seq_count):
         values = rms_scale(rows_ref[seq].astype(F32), gain)
-        tails.append(values[span - HALO :])
+        tails.append(values[span - HALO // seq_count :])
         normed = values.astype(BF16)
         for part in range(slices):
             normed_ref[part, seq * span : (seq + 1) * span, :] = normed[
@@ -427,8 +427,11 @@
     for seq in range(seq_count):
         first = seq * (HALO + span)
         rows = pl.ds(seq * span, span)
-        before = seq_count * span + seq * HALO
-        rec_ref[first : first + HALO, :] = rec_in[before : before + HALO] * kept
+        tail_rows = HALO // seq_count
+        before = seq_count * span + seq * tail_rows
+        rec_ref[first + HALO - tail_rows : first + HALO, :] = (
+            rec_in[before : before + tail_rows] * kept
+        )
         rec_ref[first + HALO : first + HALO + span, :] = rec_in[seq * span : (seq + 1) * span]
         kv = sums[seq * span : (seq + 1) * span, :kv_width]
         key = jnp.where(lane < head_dim, kv, 0.0)
@@ -627,9 +630,8 @@
                 after_refs[1][line, :] = total
                 after_refs[2][line, :] = value
                 continue
-            attended = value * (1.0 / total)
-            mean = lane_sums(attended * attended, head_dim) * (1.0 / head_dim)
-            outs.append(attended * lax.rsqrt(mean + norm_eps))
+            mean = lane_sums(value * value, head_dim) * (1.0 / head_dim)
+            outs.append(value * lax.rsqrt(mean + norm_eps * (total * total)))
         for pair in range(len(outs) // 2):
             lanes = slice(pair * width, (pair + 1) * width)
             joined = jnp.where(
@@ -710,7 +712,7 @@
         norm_kernel,
         [
             jax.ShapeDtypeStruct((count, rows, slice_width), BF16),
-            jax.ShapeDtypeStruct((count, seq_count * HALO, slice_width), BF16),
+            jax.ShapeDtypeStruct((count, HALO, slice_width), BF16),
             jax.ShapeDtypeStruct((channels, 2 * channels), BF16),
             jax.ShapeDtypeStruct((16, channels), F32),
         ],
@@ -751,7 +753,7 @@
         columns = ring.blocks[0].shape[1]
         return call(
             functools.partial(part_kernel, count, len(halos)),
-            jax.ShapeDtypeStruct((rows + len(halos) * seq_count * HALO, columns), F32),
+            jax.ShapeDtypeStruct((rows + len(halos) * HALO, columns), F32),
             [normed, *halos, *ring.blocks[:-1]],
         )
 
@@ -833,7 +835,9 @@
     att_parts = tp_spread(att_normed, tp_count)
     near, far = range(tp_count // 2), range(tp_count // 2, tp_count)
     base = project(range(tp_count), near, None, F32)
-    mixed = project((), far, base, BF16)
+    if len(far) > 1:
+        base = project((), far[:1], base, F32)
+    mixed = project((), far[-1:], base, BF16)
     return mixed.reshape(seq_count, span, out_cols)
 
 
@@ -846,7 +850,8 @@
     head_dim, rec_in_weight = arrays[5].shape[0], arrays[8]
     count, tp_count = lax.axis_size("sp"), lax.axis_size("tp")
     whole_blocks = (
-        inputs.shape[0] * rec_in_weight.shape[1] == 8 * head_dim
+        inputs.shape[0] == 2
+        and rec_in_weight.shape[1] == 4 * head_dim
         and inputs.shape[1] == 2 * head_dim
         and key_weight.shape[1] == head_dim
         and query_weight.shape[1] == rec_in_weight.shape[1]

time: 77.4 us -> 79.8 us (1.031)
  waiting for transfers between devices: 27.5 us -> 28.7 us
  starting transfers between devices: 37.8 us -> 38.9 us
    ppermute x14, waiting for transfers between devices: 10.7 us -> 7.33 us  [step(): self.behind = lax.ppermute(self.behind, 'sp', self.backward)]
    ppermute x14, starting transfers between devices: 7.4 us -> 10.5 us  [step(): self.behind = lax.ppermute(self.behind, 'sp', self.backward)]
    ppermute x6, waiting for transfers between devices: 3.61 us -> 5.99 us  [tp_spread(): found[member ^ bit] = lax.ppermute(found[member], 'tp', pairs)]
    ppermute x3, waiting for transfers between devices: 0.01 us -> 2.39 us  [ring_body(): out_weight[member] = lax.ppermute(out_weight[member], 'tp', pairs)]
    ppermute x14, starting transfers between devices: 23.2 us -> 21.1 us  [step(): self.ahead = lax.ppermute(self.ahead, 'sp', self.forward)]
    pallas_call x13 -> x14, Pallas kernels: 10.1 us -> 10.1 us  [call(): pl.pallas_call(kernel, out_shape=outs if single else tuple(outs), in_spec...]
  transfers between devices with their start and end apart: 38 -> 38, of which waited for: 15 -> 15; matrix products, arithmetic and copies ran while one was open for 0% -> 0% of each run, Pallas kernels for 12% -> 11%
where the time goes in v2:
time: 79.8 us; the launch traced here: 79.6 us
  starting transfers between devices  38.9 us (49%)
  waiting for transfers between devices  28.7 us (36%)
  Pallas kernels  10.1 us (13%)
  local copies, waits for them, and re-layouts  1.63 us (2%)
    ppermute x14, starting transfers between devices, step(): self.ahead = lax.ppermute(self.ahead, 'sp', self.forward)  21.1 us
    ppermute x14, starting transfers between devices, step(): self.behind = lax.ppermute(self.behind, 'sp', self.backward)  10.5 us
    pallas_call x14, Pallas kernels, call(): pl.pallas_call(kernel, out_shape=outs if single else tuple(outs), in_spec...  10.1 us
    ppermute x14, waiting for transfers between devices, step(): self.ahead = lax.ppermute(self.ahead, 'sp', self.forward)  9.51 us
    ppermute x14, waiting for transfers between devices, step(): self.behind = lax.ppermute(self.behind, 'sp', self.backward)  7.33 us
    ppermute x6, waiting for transfers between devices, tp_spread(): found[member ^ bit] = lax.ppermute(found[member], 'tp', pairs)  5.99 us
    ppermute x1, waiting for transfers between devices, ring_body(): halo = lax.ppermute(tail, 'sp', shift)  3.51 us
    ppermute x3, starting transfers between devices, ring_body(): out_weight[member] = lax.ppermute(out_weight[member], 'tp', pairs)  3.03 us
  transfers between devices with their start and end apart: 38, of which 15 were waited for; matrix products, arithmetic and copies ran while one was open for 0% of the time, Pallas kernels for 11%

profile of v2, /device:TPU:0, one launch (start us, length us, event | category | flops | bytes accessed | tf_op | source)
XLA Modules:
  0.0 79.6 jit_solution(2273472022858832968)
XLA Ops:
  1.1 3.1 %collective-permute-start.8 = (bf16[256,384]{1,0:T(8,128)(2,1)S(1)}, bf16[256,384]{1,0:T(8,128)(2,1)S(1)}, u32[]{:S(2)}, u32[]{:S(2)}) collective-permute-start(bf16[256,384]{1,0:T(8,128)(2,1)S(1)} %shard_map.184.refs_1_), channel_id=1, source_target_pairs={{0,8},{8,16},{16,24},{24,28},{28,20},{20,12},{12,4},{4,0},{1,9},{9... | collective-permute-start | bytes 589832 | tf_op jit(solution)/shard_map/ppermute | solution.py:277
  4.2 2.0 %collective-permute-start.27 = (bf16[256,256]{1,0:T(8,128)(2,1)S(1)}, bf16[256,256]{1,0:T(8,128)(2,1)S(1)}, u32[]{:S(2)}, u32[]{:S(2)}) collective-permute-start(bf16[256,256]{1,0:T(8,128)(2,1)S(1)} %copy-done.5), channel_id=1, source_target_pairs={{8,0},{16,8},{24,16},{28,24},{20,28},{12,20},{4,12},{0,4},{9,1},{1... | collective-permute-start | bytes 393224 | tf_op jit(solution)/shard_map/ppermute | solution.py:280
  6.2 2.9 %collective-permute-done.8.refs_2_ = bf16[256,384]{1,0:T(8,128)(2,1)S(1)} collective-permute-done((bf16[256,384]{1,0:T(8,128)(2,1)S(1)}, bf16[256,384]{1,0:T(8,128)(2,1)S(1)}, u32[]{:S(2)}, u32[]{:S(2)}) %collective-permute-start.8) | collective-permute-done | bytes 196640 | tf_op jit(solution)/shard_map/ppermute | solution.py:277
  9.1 1.8 %collective-permute-start.10 = (bf16[256,384]{1,0:T(8,128)(2,1)S(1)}, bf16[256,384]{1,0:T(8,128)(2,1)S(1)}, u32[]{:S(2)}, u32[]{:S(2)}) collective-permute-start(bf16[256,384]{1,0:T(8,128)(2,1)S(1)} %collective-permute-done.8.refs_2_), channel_id=1, source_target_pairs={{0,8},{8,16},{16,24},{24,28},{28,20},{20,12},{12,4},{4,0},{1,9},{9... | collective-permute-start | bytes 589832 | tf_op jit(solution)/shard_map/ppermute | solution.py:277
  13.2 2.0 %collective-permute-start.7 = (bf16[8,8,256]{2,1,0:T(8,128)(2,1)S(1)}, bf16[8,8,256]{2,1,0:T(8,128)(2,1)S(1)}, u32[]{:S(2)}, u32[]{:S(2)}) collective-permute-start(bf16[8,8,256]{2,1,0:T(8,128)(2,1)S(1)} %get-tuple-element.21), channel_id=1, source_target_pairs={{0,4},{4,8},{8,12},{12,16},{16,20},{20,24},{24,28},{28,0},{1,5},{5... | collective-permute-start | bytes 98312 | tf_op jit(solution)/shard_map/ppermute | solution.py:740
  15.2 1.6 %collective-permute-start.26 = (bf16[256,256]{1,0:T(8,128)(2,1)S(1)}, bf16[256,256]{1,0:T(8,128)(2,1)S(1)}, u32[]{:S(2)}, u32[]{:S(2)}) collective-permute-start(bf16[256,256]{1,0:T(8,128)(2,1)S(1)} %copy-done.5), channel_id=1, source_target_pairs={{0,8},{8,16},{16,24},{24,28},{28,20},{20,12},{12,4},{4,0},{1,9},{9... | collective-permute-start | bytes 393224 | tf_op jit(solution)/shard_map/ppermute | solution.py:277
  16.8 3.5 %collective-permute-done.7.refs_0_.refs_1_ = bf16[8,8,256]{2,1,0:T(8,128)(2,1)S(1)} collective-permute-done((bf16[8,8,256]{2,1,0:T(8,128)(2,1)S(1)}, bf16[8,8,256]{2,1,0:T(8,128)(2,1)S(1)}, u32[]{:S(2)}, u32[]{:S(2)}) %collective-permute-start.7) | collective-permute-done | bytes 32800 | tf_op jit(solution)/shard_map/ppermute | solution.py:740
  20.3 2.0 %collective-permute-start = (bf16[256,256]{1,0:T(8,128)(2,1)S(1)}, bf16[256,256]{1,0:T(8,128)(2,1)S(1)}, u32[]{:S(2)}, u32[]{:S(2)}) collective-permute-start(bf16[256,256]{1,0:T(8,128)(2,1)S(1)} %copy-done.6), channel_id=1, source_target_pairs={{0,8},{8,16},{16,24},{24,28},{28,20},{20,12},{12,4},{4,0},{1,9},{9... | collective-permute-start | bytes 393224 | tf_op jit(solution)/shard_map/ppermute | solution.py:277
  22.4 1.9 %collective-permute-start.13 = (bf16[256,384]{1,0:T(8,128)(2,1)S(1)}, bf16[256,384]{1,0:T(8,128)(2,1)S(1)}, u32[]{:S(2)}, u32[]{:S(2)}) collective-permute-start(bf16[256,384]{1,0:T(8,128)(2,1)S(1)} %collective-permute-done.11.refs_5_), channel_id=1, source_target_pairs={{8,0},{16,8},{24,16},{28,24},{20,28},{12,20},{4,12},{0,4},{9,1},{1... | collective-permute-start | bytes 589832 | tf_op jit(solution)/shard_map/ppermute | solution.py:280
  24.4 2.2 %collective-permute-done.1.refs_2_ = bf16[256,256]{1,0:T(8,128)(2,1)S(1)} collective-permute-done((bf16[256,256]{1,0:T(8,128)(2,1)S(1)}, bf16[256,256]{1,0:T(8,128)(2,1)S(1)}, u32[]{:S(2)}, u32[]{:S(2)}) %collective-permute-start.1) | collective-permute-done | bytes 131104 | tf_op jit(solution)/shard_map/ppermute | solution.py:280
  26.8 1.9 %collective-permute-start.3 = (bf16[256,256]{1,0:T(8,128)(2,1)S(1)}, bf16[256,256]{1,0:T(8,128)(2,1)S(1)}, u32[]{:S(2)}, u32[]{:S(2)}) collective-permute-start(bf16[256,256]{1,0:T(8,128)(2,1)S(1)} %collective-permute-done.1.refs_2_), channel_id=1, source_target_pairs={{8,0},{16,8},{24,16},{28,24},{20,28},{12,20},{4,12},{0,4},{9,1},{1... | collective-permute-start | bytes 393224 | tf_op jit(solution)/shard_map/ppermute | solution.py:280
  28.7 3.2 %collective-permute-done.29.refs_4_ = bf16[256,256]{1,0:T(8,128)(2,1)S(1)} collective-permute-done((bf16[256,256]{1,0:T(8,128)(2,1)S(1)}, bf16[256,256]{1,0:T(8,128)(2,1)S(1)}, u32[]{:S(2)}, u32[]{:S(2)}) %collective-permute-start.29) | collective-permute-done | bytes 131104 | tf_op jit(solution)/shard_map/ppermute | solution.py:280
  31.8 1.6 %collective-permute-start.2 = (bf16[256,256]{1,0:T(8,128)(2,1)S(1)}, bf16[256,256]{1,0:T(8,128)(2,1)S(1)}, u32[]{:S(2)}, u32[]{:S(2)}) collective-permute-start(bf16[256,256]{1,0:T(8,128)(2,1)S(1)} %collective-permute-done.refs_1_), channel_id=1, source_target_pairs={{0,8},{8,16},{16,24},{24,28},{28,20},{20,12},{12,4},{4,0},{1,9},{9... | collective-permute-start | bytes 393224 | tf_op jit(solution)/shard_map/ppermute | solution.py:277
  34.6 1.6 %collective-permute-start.30 = (bf16[256,256]{1,0:T(8,128)(2,1)S(1)}, bf16[256,256]{1,0:T(8,128)(2,1)S(1)}, u32[]{:S(2)}, u32[]{:S(2)}) collective-permute-start(bf16[256,256]{1,0:T(8,128)(2,1)S(1)} %collective-permute-done.28.refs_3_), channel_id=1, source_target_pairs={{0,8},{8,16},{16,24},{24,28},{28,20},{20,12},{12,4},{4,0},{1,9},{9... | collective-permute-start | bytes 393224 | tf_op jit(solution)/shard_map/ppermute | solution.py:277
  36.8 1.6 %collective-permute-start.14 = (bf16[256,384]{1,0:T(8,128)(2,1)S(1)}, bf16[256,384]{1,0:T(8,128)(2,1)S(1)}, u32[]{:S(2)}, u32[]{:S(2)}) collective-permute-start(bf16[256,384]{1,0:T(8,128)(2,1)S(1)} %collective-permute-done.12.refs_6_), channel_id=1, source_target_pairs={{0,8},{8,16},{16,24},{24,28},{28,20},{20,12},{12,4},{4,0},{1,9},{9... | collective-permute-start | bytes 589832 | tf_op jit(solution)/shard_map/ppermute | solution.py:277
  39.1 3.5 %collective-permute-done.14.refs_3_ = bf16[256,384]{1,0:T(8,128)(2,1)S(1)} collective-permute-done((bf16[256,384]{1,0:T(8,128)(2,1)S(1)}, bf16[256,384]{1,0:T(8,128)(2,1)S(1)}, u32[]{:S(2)}, u32[]{:S(2)}) %collective-permute-start.14) | collective-permute-done | bytes 196640 | tf_op jit(solution)/shard_map/ppermute | solution.py:277
  46.3 1.6 %collective-permute-start.4 = (bf16[256,256]{1,0:T(8,128)(2,1)S(1)}, bf16[256,256]{1,0:T(8,128)(2,1)S(1)}, u32[]{:S(2)}, u32[]{:S(2)}) collective-permute-start(bf16[256,256]{1,0:T(8,128)(2,1)S(1)} %collective-permute-done.2.refs_3_), channel_id=1, source_target_pairs={{0,8},{8,16},{16,24},{24,28},{28,20},{20,12},{12,4},{4,0},{1,9},{9... | collective-permute-start | bytes 393224 | tf_op jit(solution)/shard_map/ppermute | solution.py:277
  51.9 2.3 %collective-permute-start.25 = (bf16[512,512]{1,0:T(8,128)(2,1)S(1)}, bf16[512,512]{1,0:T(8,128)(2,1)S(1)}, u32[]{:S(2)}, u32[]{:S(2)}) collective-permute-start(bf16[512,512]{1,0:T(8,128)(2,1)S(1)} %get-tuple-element.28), channel_id=1, source_target_pairs={{0,2},{1,3},{2,0},{3,1},{4,6},{5,7},{6,4},{7,5},{8,10},{9,11},{10,... | collective-permute-start | bytes 1572872 | tf_op jit(solution)/shard_map/ppermute | solution.py:743
  54.9 1.7 %collective-permute-start.17 = (bf16[288,128]{1,0:T(8,128)(2,1)S(1)}, bf16[288,128]{1,0:T(8,128)(2,1)S(1)}, u32[]{:S(2)}, u32[]{:S(2)}) collective-permute-start(bf16[288,128]{1,0:T(8,128)(2,1)S(1)} %collective-permute-done.16.refs_4_.refs_3_), channel_id=1, source_target_pairs={{0,8},{8,16},{16,24},{24,28},{28,20},{20,12},{12,4},{4,0},{1,9},{9... | collective-permute-start | bytes 221192 | tf_op jit(solution)/shard_map/ppermute | solution.py:277
  59.3 1.6 %collective-permute-start.32 = (bf16[256,256]{1,0:T(8,128)(2,1)S(1)}, bf16[256,256]{1,0:T(8,128)(2,1)S(1)}, u32[]{:S(2)}, u32[]{:S(2)}) collective-permute-start(bf16[256,256]{1,0:T(8,128)(2,1)S(1)} %collective-permute-done.31.refs_6_), channel_id=1, source_target_pairs={{8,0},{16,8},{24,16},{28,24},{20,28},{12,20},{4,12},{0,4},{9,1},{1... | collective-permute-start | bytes 393224 | tf_op jit(solution)/shard_map/ppermute | solution.py:280
  62.2 2.5 %shard_map.187 = (f32[1024,128]{1,0:T(8,128)S(1)}, f32[1024,128]{1,0:T(8,128)S(1)}, f32[1024,128]{1,0:T(8,128)S(1)}) custom-call(bf16[8,128,128]{2,1,0:T(8,128)(2,1)S(1)} %shard_map.182.refs_0_, bf16[288,128]{1,0:T(8,128)(2,1)S(1)} %get-tuple-element.23.refs_1_.refs_0_, bf16[288,128]{1,0:T(8,128)(2,1)S(1)} %collective-permute-done.15.refs_2_.refs_1_, ...), custom_call_target="tpu_custom_call" | custom-call | flops 4000000000 | tf_op jit(solution)/shard_map/pallas_call | solution.py:290
  69.4 2.4 %collective-permute-done.25.refs_8_.refs_1_ = bf16[512,512]{1,0:T(8,128)(2,1)S(1)} collective-permute-done((bf16[512,512]{1,0:T(8,128)(2,1)S(1)}, bf16[512,512]{1,0:T(8,128)(2,1)S(1)}, u32[]{:S(2)}, u32[]{:S(2)}) %collective-permute-start.25) | collective-permute-done | bytes 524320 | tf_op jit(solution)/shard_map/ppermute | solution.py:743
  71.8 2.8 %collective-permute-done.34.refs_2_ = bf16[256,256]{1,0:T(8,128)(2,1)S(1)} collective-permute-done((bf16[256,256]{1,0:T(8,128)(2,1)S(1)}, bf16[256,256]{1,0:T(8,128)(2,1)S(1)}, u32[]{:S(2)}, u32[]{:S(2)}) %collective-permute-start.34) | collective-permute-done | bytes 131104 | tf_op jit(solution)/shard_map/ppermute | solution.py:664
  74.6 2.7 %collective-permute-done.22.refs_0_ = bf16[256,256]{1,0:T(8,128)(2,1)S(1)} collective-permute-done((bf16[256,256]{1,0:T(8,128)(2,1)S(1)}, bf16[256,256]{1,0:T(8,128)(2,1)S(1)}, u32[]{:S(2)}, u32[]{:S(2)}) %collective-permute-start.22) | collective-permute-done | bytes 131104 | tf_op jit(solution)/shard_map/ppermute | solution.py:664
  (104 shorter events, 25.5 us)
Async XLA Ops:
  1.1 7.9 %collective-permute-start.8 = (bf16[256,384]{1,0:T(8,128)(2,1)S(1)}, bf16[256,384]{1,0:T(8,128)(2,1)S(1)}, u32[]{:S(2)}, u32[]{:S(2)}) collective-permute-start(bf16[256,384]{1,0:T(8,128)(2,1)S(1)} %shard_map.184.refs_1_), channel_id=1, source_target_pairs={{0,8},{8,16},{16,24},{24,28},{28,20},{20,12},{12,4},{4,0},{1,9},{9... | collective-permute-start | bytes 589832 | tf_op jit(solution)/shard_map/ppermute | solution.py:277
  4.2 7.8 %collective-permute-start.9 = (bf16[256,384]{1,0:T(8,128)(2,1)S(1)}, bf16[256,384]{1,0:T(8,128)(2,1)S(1)}, u32[]{:S(2)}, u32[]{:S(2)}) collective-permute-start(bf16[256,384]{1,0:T(8,128)(2,1)S(1)} %shard_map.184.refs_1_), channel_id=1, source_target_pairs={{8,0},{16,8},{24,16},{28,24},{20,28},{12,20},{4,12},{0,4},{9,1},{1... | collective-permute-start | bytes 589832 | tf_op jit(solution)/shard_map/ppermute | solution.py:280
  4.2 16.0 %collective-permute-start.27 = (bf16[256,256]{1,0:T(8,128)(2,1)S(1)}, bf16[256,256]{1,0:T(8,128)(2,1)S(1)}, u32[]{:S(2)}, u32[]{:S(2)}) collective-permute-start(bf16[256,256]{1,0:T(8,128)(2,1)S(1)} %copy-done.5), channel_id=1, source_target_pairs={{8,0},{16,8},{24,16},{28,24},{20,28},{12,20},{4,12},{0,4},{9,1},{1... | collective-permute-start | bytes 393224 | tf_op jit(solution)/shard_map/ppermute | solution.py:280
  9.1 13.2 %collective-permute-start.10 = (bf16[256,384]{1,0:T(8,128)(2,1)S(1)}, bf16[256,384]{1,0:T(8,128)(2,1)S(1)}, u32[]{:S(2)}, u32[]{:S(2)}) collective-permute-start(bf16[256,384]{1,0:T(8,128)(2,1)S(1)} %collective-permute-done.8.refs_2_), channel_id=1, source_target_pairs={{0,8},{8,16},{16,24},{24,28},{28,20},{20,12},{12,4},{4,0},{1,9},{9... | collective-permute-start | bytes 589832 | tf_op jit(solution)/shard_map/ppermute | solution.py:277
  12.0 10.5 %collective-permute-start.11 = (bf16[256,384]{1,0:T(8,128)(2,1)S(1)}, bf16[256,384]{1,0:T(8,128)(2,1)S(1)}, u32[]{:S(2)}, u32[]{:S(2)}) collective-permute-start(bf16[256,384]{1,0:T(8,128)(2,1)S(1)} %collective-permute-done.9.refs_3_), channel_id=1, source_target_pairs={{8,0},{16,8},{24,16},{28,24},{20,28},{12,20},{4,12},{0,4},{9,1},{1... | collective-permute-start | bytes 589832 | tf_op jit(solution)/shard_map/ppermute | solution.py:280
  13.2 7.1 %collective-permute-start.7 = (bf16[8,8,256]{2,1,0:T(8,128)(2,1)S(1)}, bf16[8,8,256]{2,1,0:T(8,128)(2,1)S(1)}, u32[]{:S(2)}, u32[]{:S(2)}) collective-permute-start(bf16[8,8,256]{2,1,0:T(8,128)(2,1)S(1)} %get-tuple-element.21), channel_id=1, source_target_pairs={{0,4},{4,8},{8,12},{12,16},{16,20},{20,24},{24,28},{28,0},{1,5},{5... | collective-permute-start | bytes 98312 | tf_op jit(solution)/shard_map/ppermute | solution.py:740
  15.2 9.2 %collective-permute-start.26 = (bf16[256,256]{1,0:T(8,128)(2,1)S(1)}, bf16[256,256]{1,0:T(8,128)(2,1)S(1)}, u32[]{:S(2)}, u32[]{:S(2)}) collective-permute-start(bf16[256,256]{1,0:T(8,128)(2,1)S(1)} %copy-done.5), channel_id=1, source_target_pairs={{0,8},{8,16},{16,24},{24,28},{28,20},{20,12},{12,4},{4,0},{1,9},{9... | collective-permute-start | bytes 393224 | tf_op jit(solution)/shard_map/ppermute | solution.py:277
  22.3 13.9 %collective-permute-start.12 = (bf16[256,384]{1,0:T(8,128)(2,1)S(1)}, bf16[256,384]{1,0:T(8,128)(2,1)S(1)}, u32[]{:S(2)}, u32[]{:S(2)}) collective-permute-start(bf16[256,384]{1,0:T(8,128)(2,1)S(1)} %collective-permute-done.10.refs_4_), channel_id=1, source_target_pairs={{0,8},{8,16},{16,24},{24,28},{28,20},{20,12},{12,4},{4,0},{1,9},{9... | collective-permute-start | bytes 589832 | tf_op jit(solution)/shard_map/ppermute | solution.py:277
  22.4 14.3 %collective-permute-start.13 = (bf16[256,384]{1,0:T(8,128)(2,1)S(1)}, bf16[256,384]{1,0:T(8,128)(2,1)S(1)}, u32[]{:S(2)}, u32[]{:S(2)}) collective-permute-start(bf16[256,384]{1,0:T(8,128)(2,1)S(1)} %collective-permute-done.11.refs_5_), channel_id=1, source_target_pairs={{8,0},{16,8},{24,16},{28,24},{20,28},{12,20},{4,12},{0,4},{9,1},{1... | collective-permute-start | bytes 589832 | tf_op jit(solution)/shard_map/ppermute | solution.py:280
  24.3 7.5 %collective-permute-start.29 = (bf16[256,256]{1,0:T(8,128)(2,1)S(1)}, bf16[256,256]{1,0:T(8,128)(2,1)S(1)}, u32[]{:S(2)}, u32[]{:S(2)}) collective-permute-start(bf16[256,256]{1,0:T(8,128)(2,1)S(1)} %collective-permute-done.27.refs_2_), channel_id=1, source_target_pairs={{8,0},{16,8},{24,16},{28,24},{20,28},{12,20},{4,12},{0,4},{9,1},{1... | collective-permute-start | bytes 393224 | tf_op jit(solution)/shard_map/ppermute | solution.py:280
  26.6 6.8 %collective-permute-start.28 = (bf16[256,256]{1,0:T(8,128)(2,1)S(1)}, bf16[256,256]{1,0:T(8,128)(2,1)S(1)}, u32[]{:S(2)}, u32[]{:S(2)}) collective-permute-start(bf16[256,256]{1,0:T(8,128)(2,1)S(1)} %collective-permute-done.26.refs_1_), channel_id=1, source_target_pairs={{0,8},{8,16},{16,24},{24,28},{28,20},{20,12},{12,4},{4,0},{1,9},{9... | collective-permute-start | bytes 393224 | tf_op jit(solution)/shard_map/ppermute | solution.py:277
  26.8 7.9 %collective-permute-start.3 = (bf16[256,256]{1,0:T(8,128)(2,1)S(1)}, bf16[256,256]{1,0:T(8,128)(2,1)S(1)}, u32[]{:S(2)}, u32[]{:S(2)}) collective-permute-start(bf16[256,256]{1,0:T(8,128)(2,1)S(1)} %collective-permute-done.1.refs_2_), channel_id=1, source_target_pairs={{8,0},{16,8},{24,16},{28,24},{20,28},{12,20},{4,12},{0,4},{9,1},{1... | collective-permute-start | bytes 393224 | tf_op jit(solution)/shard_map/ppermute | solution.py:280
  31.8 13.6 %collective-permute-start.2 = (bf16[256,256]{1,0:T(8,128)(2,1)S(1)}, bf16[256,256]{1,0:T(8,128)(2,1)S(1)}, u32[]{:S(2)}, u32[]{:S(2)}) collective-permute-start(bf16[256,256]{1,0:T(8,128)(2,1)S(1)} %collective-permute-done.refs_1_), channel_id=1, source_target_pairs={{0,8},{8,16},{16,24},{24,28},{28,20},{20,12},{12,4},{4,0},{1,9},{9... | collective-permute-start | bytes 393224 | tf_op jit(solution)/shard_map/ppermute | solution.py:277
  33.4 12.8 %collective-permute-start.31 = (bf16[256,256]{1,0:T(8,128)(2,1)S(1)}, bf16[256,256]{1,0:T(8,128)(2,1)S(1)}, u32[]{:S(2)}, u32[]{:S(2)}) collective-permute-start(bf16[256,256]{1,0:T(8,128)(2,1)S(1)} %collective-permute-done.29.refs_4_), channel_id=1, source_target_pairs={{8,0},{16,8},{24,16},{28,24},{20,28},{12,20},{4,12},{0,4},{9,1},{1... | collective-permute-start | bytes 393224 | tf_op jit(solution)/shard_map/ppermute | solution.py:280
  34.6 11.6 %collective-permute-start.30 = (bf16[256,256]{1,0:T(8,128)(2,1)S(1)}, bf16[256,256]{1,0:T(8,128)(2,1)S(1)}, u32[]{:S(2)}, u32[]{:S(2)}) collective-permute-start(bf16[256,256]{1,0:T(8,128)(2,1)S(1)} %collective-permute-done.28.refs_3_), channel_id=1, source_target_pairs={{0,8},{8,16},{16,24},{24,28},{28,20},{20,12},{12,4},{4,0},{1,9},{9... | collective-permute-start | bytes 393224 | tf_op jit(solution)/shard_map/ppermute | solution.py:277
  36.2 11.6 %collective-permute-start.5 = (bf16[256,256]{1,0:T(8,128)(2,1)S(1)}, bf16[256,256]{1,0:T(8,128)(2,1)S(1)}, u32[]{:S(2)}, u32[]{:S(2)}) collective-permute-start(bf16[256,256]{1,0:T(8,128)(2,1)S(1)} %collective-permute-done.3.refs_4_), channel_id=1, source_target_pairs={{8,0},{16,8},{24,16},{28,24},{20,28},{12,20},{4,12},{0,4},{9,1},{1... | collective-permute-start | bytes 393224 | tf_op jit(solution)/shard_map/ppermute | solution.py:280
  46.2 23.2 %collective-permute-start.24 = (bf16[512,512]{1,0:T(8,128)(2,1)S(1)}, bf16[512,512]{1,0:T(8,128)(2,1)S(1)}, u32[]{:S(2)}, u32[]{:S(2)}) collective-permute-start(bf16[512,512]{1,0:T(8,128)(2,1)S(1)} %get-tuple-element.27), channel_id=1, source_target_pairs={{0,3},{1,2},{2,1},{3,0},{4,7},{5,6},{6,5},{7,4},{8,11},{9,10},{10,... | collective-permute-start | bytes 1572872 | tf_op jit(solution)/shard_map/ppermute | solution.py:743
  48.4 6.5 %collective-permute-start.16 = (bf16[288,128]{1,0:T(8,128)(2,1)S(1)}, bf16[288,128]{1,0:T(8,128)(2,1)S(1)}, u32[]{:S(2)}, u32[]{:S(2)}) collective-permute-start(bf16[288,128]{1,0:T(8,128)(2,1)S(1)} %collective-permute-done.15.refs_2_.refs_1_), channel_id=1, source_target_pairs={{0,8},{8,16},{16,24},{24,28},{28,20},{20,12},{12,4},{4,0},{1,9},{9... | collective-permute-start | bytes 221192 | tf_op jit(solution)/shard_map/ppermute | solution.py:277
  49.9 6.7 %collective-permute-start.20 = (bf16[288,128]{1,0:T(8,128)(2,1)S(1)}, bf16[288,128]{1,0:T(8,128)(2,1)S(1)}, u32[]{:S(2)}, u32[]{:S(2)}) collective-permute-start(bf16[288,128]{1,0:T(8,128)(2,1)S(1)} %collective-permute-done.19.refs_3_.refs_2_), channel_id=1, source_target_pairs={{8,0},{16,8},{24,16},{28,24},{20,28},{12,20},{4,12},{0,4},{9,1},{1... | collective-permute-start | bytes 221192 | tf_op jit(solution)/shard_map/ppermute | solution.py:280
  51.9 19.8 %collective-permute-start.25 = (bf16[512,512]{1,0:T(8,128)(2,1)S(1)}, bf16[512,512]{1,0:T(8,128)(2,1)S(1)}, u32[]{:S(2)}, u32[]{:S(2)}) collective-permute-start(bf16[512,512]{1,0:T(8,128)(2,1)S(1)} %get-tuple-element.28), channel_id=1, source_target_pairs={{0,2},{1,3},{2,0},{3,1},{4,6},{5,7},{6,4},{7,5},{8,10},{9,11},{10,... | collective-permute-start | bytes 1572872 | tf_op jit(solution)/shard_map/ppermute | solution.py:743
  54.2 23.2 %collective-permute-start.37 = (bf16[512,512]{1,0:T(8,128)(2,1)S(1)}, bf16[512,512]{1,0:T(8,128)(2,1)S(1)}, u32[]{:S(2)}, u32[]{:S(2)}) collective-permute-start(bf16[512,512]{1,0:T(8,128)(2,1)S(1)} %get-tuple-element.32), channel_id=1, source_target_pairs={{0,1},{1,0},{2,3},{3,2},{4,5},{5,4},{6,7},{7,6},{8,9},{9,8},{10,11... | collective-permute-start | bytes 1572872 | tf_op jit(solution)/shard_map/ppermute | solution.py:743
  65.8 8.8 %collective-permute-start.34 = (bf16[256,256]{1,0:T(8,128)(2,1)S(1)}, bf16[256,256]{1,0:T(8,128)(2,1)S(1)}, u32[]{:S(2)}, u32[]{:S(2)}) collective-permute-start(bf16[256,256]{1,0:T(8,128)(2,1)S(1)} %shard_map.191.refs_0_), channel_id=1, source_target_pairs={{0,2},{1,3},{2,0},{3,1},{4,6},{5,7},{6,4},{7,5},{8,10},{9,11},{10,... | collective-permute-start | bytes 393224 | tf_op jit(solution)/shard_map/ppermute | solution.py:664
  68.4 8.9 %collective-permute-start.22 = (bf16[256,256]{1,0:T(8,128)(2,1)S(1)}, bf16[256,256]{1,0:T(8,128)(2,1)S(1)}, u32[]{:S(2)}, u32[]{:S(2)}) collective-permute-start(bf16[256,256]{1,0:T(8,128)(2,1)S(1)} %shard_map.188.refs_4_), channel_id=1, source_target_pairs={{0,2},{1,3},{2,0},{3,1},{4,6},{5,7},{6,4},{7,5},{8,10},{9,11},{10,... | collective-permute-start | bytes 393224 | tf_op jit(solution)/shard_map/ppermute | solution.py:664
  69.4 8.0 %collective-permute-start.33 = (bf16[256,256]{1,0:T(8,128)(2,1)S(1)}, bf16[256,256]{1,0:T(8,128)(2,1)S(1)}, u32[]{:S(2)}, u32[]{:S(2)}) collective-permute-start(bf16[256,256]{1,0:T(8,128)(2,1)S(1)} %shard_map.191.refs_0_), channel_id=1, source_target_pairs={{0,1},{1,0},{2,3},{3,2},{4,5},{5,4},{6,7},{7,6},{8,9},{9,8},{10,11... | collective-permute-start | bytes 393224 | tf_op jit(solution)/shard_map/ppermute | solution.py:664
  (33 other events, 190.2 us)
